TPU v7x, 256 devices: a whole 4x4x8 slice. The times are simulated.
256 devices in a mesh: sp: 64 (over z, y, core), tp: 4 (over x).
Axes of the slice: x: 4, y: 4, z: 8, core: 2. Of those that a mesh axis runs over, the one named last changes fastest.
Arguments:
- resid_in: bfloat16 [16384, 2048], P(('sp', 'tp')), may hold values from -6 to 6
- query_proj: bfloat16 [16384, 512], P('sp', 'tp'), may hold values from -6 to 6
- key_proj: bfloat16 [16384, 256], P('sp', 'tp'), may hold values from -6 to 6
- value_proj: bfloat16 [16384, 256], P('sp', 'tp'), may hold values from -6 to 6
- query_gain: float32 [8, 64], P('tp'), may hold values from 0.5 to 6
- key_gain: float32 [4, 64], P('tp'), may hold values from 0.5 to 6
- out_weight: bfloat16 [512, 2048], replicated, may hold values from -0.25 to 0.25
- norm_gain: float32 [2048], replicated, may hold values from 0.1 to 1.9
- gate_weight: bfloat16 [64, 2048, 1024], P('sp', None, 'tp'), may hold values from -0.125 to 0.125
- up_weight: bfloat16 [64, 2048, 1024], P('sp', None, 'tp'), may hold values from -0.125 to 0.125
- down_weight: bfloat16 [64, 1024, 2048], P('sp', 'tp'), may hold values from -0.1875 to 0.1875
- expert_ids: int32 [16384, 2], P('sp'), may hold values from 0 to 63, all different within a row; in each aligned block of 64 rows (0 to 63, 64 to 127, ...) at most 3 rows name the same one
- route_weight: float32 [16384, 2], P(('sp', 'tp')), may hold values from 0.2 to 1
Outputs:
- layer_out: bfloat16 [16384, 2048], P(('sp', 'tp'))
Inputs may be any that keep to these rules, and one draw needn't show every extreme that they name: `expert_ids`: each row names 2 different experts. In each aligned block of rows that one device holds (rows of one index of sp and tp together), no expert is named more than 3 times, and in some blocks one expert is named exactly 3 times.
All inputs are finite; a program needn't handle non-finite values.
Results may differ from a plain program's by a relative error of at most 0.014.
Values may be sent and summed in bfloat16 or wider, within the bound.
A program may use at most 64 MiB of HBM per device.

v0:
```python
import jax
import jax.numpy as jnp
from jax import lax
from jax.sharding import PartitionSpec as P

HEAD_DIM = 64
TOPK = 2
GRID_W = 64
TOK_DEV = 256


eps = 1e-06
rope_base = 10000.0


def side_by_side(arrays, axis, dim, along):
    both = jnp.concatenate(arrays, axis=along)
    filled, at, gathered = (lax.all_gather(both, axis, axis=dim, tiled=True), 0, [])
    for a in arrays:
        gathered.append(lax.slice_in_dim(filled, at, at + a.shape[along], axis=along))
        at += a.shape[along]
    return tuple(gathered)


def joined_along(tiles, dim):
    dims = list(tiles.shape[1:])
    dims[dim] *= tiles.shape[0]
    return jnp.moveaxis(tiles, 0, dim).reshape(dims)


def work_in_pieces(value, axis, dim, apply, out_dim):
    devices, width = (lax.axis_size(axis), value.shape[dim])
    count = 2 if width % 2 == 0 else 1
    gathered, length = ([], width // count)
    for k in range(count):
        piece = lax.slice_in_dim(value, k * length, (k + 1) * length, axis=dim)
        starts = jnp.arange(devices) * width + k * length
        gathered.append(jax.vmap(apply)(lax.all_gather(piece, axis), starts))
    return joined_along(jnp.concatenate(gathered, axis=out_dim + 1), out_dim)


def in_blocks(value, dim, devices):
    before, after = (value.shape[:dim], value.shape[dim + 1 :])
    return jnp.moveaxis(value.reshape(*before, devices, -1, *after), dim, 0)


def summed_on_arrival(value, axis, dim):
    devices = lax.axis_size(axis)
    tiles = lax.all_to_all(in_blocks(value, dim, devices), axis, 0, 0, tiled=True)
    return jnp.sum(tiles.astype(jnp.float32), axis=0)


def rotary_tables(positions):
    row_pos = (positions // GRID_W).astype(jnp.float32)
    col_pos = (positions % GRID_W).astype(jnp.float32)
    freq_count = HEAD_DIM // 4
    inverse = rope_base ** (-jnp.arange(freq_count, dtype=jnp.float32) / freq_count)
    angles = jnp.concatenate([row_pos[:, None] * inverse, col_pos[:, None] * inverse], axis=-1)
    return (jnp.cos(angles), jnp.sin(angles))


def prepare(projected, gains, cosine, sine_table):
    tok_total = projected.shape[0]
    head_count = gains.shape[0]
    values_f = projected.astype(jnp.float32).reshape(tok_total, head_count, HEAD_DIM)
    normed = (
        values_f
        * lax.rsqrt(jnp.mean(values_f * values_f, axis=-1, keepdims=True) + eps)
        * gains[None]
    )
    half_dim = HEAD_DIM // 2
    first_half = normed[..., :half_dim]
    second_half = normed[..., half_dim:]
    cos_b = cosine[:, None, :]
    sin_b = sine_table[:, None, :]
    rotated = jnp.concatenate(
        [first_half * cos_b - second_half * sin_b, second_half * cos_b + first_half * sin_b],
        axis=-1,
    )
    return rotated.astype(jnp.bfloat16)


def slot_index(ids_rows, expert_count, capacity):
    flat_ids = ids_rows.reshape(-1)
    member = (flat_ids[:, None] == jnp.arange(expert_count, dtype=jnp.int32)[None, :]).astype(
        jnp.int32
    )
    ranks = jnp.sum((jnp.cumsum(member, axis=0) - member) * member, axis=1)
    return flat_ids * capacity + ranks


def build_send(rows, ids_rows, expert_count, capacity):
    slot_ids = slot_index(ids_rows, expert_count, capacity)
    picker = (
        jnp.arange(expert_count * capacity, dtype=jnp.int32)[:, None] == slot_ids[None, :]
    ).astype(jnp.bfloat16)
    repeated = jnp.repeat(rows, ids_rows.shape[1], axis=0)
    outgoing = jnp.dot(picker, repeated, preferred_element_type=jnp.float32).astype(jnp.bfloat16)
    return outgoing.reshape(expert_count, capacity, rows.shape[1])


def expert_ffn(rows, gate_local, up_local, down_local):
    lead_shape = rows.shape[:-1]
    flat_rows = rows.reshape(-1, rows.shape[-1])
    gate = jnp.dot(flat_rows, gate_local, preferred_element_type=jnp.float32)
    upper = jnp.dot(flat_rows, up_local, preferred_element_type=jnp.float32)
    hidden = (jax.nn.silu(gate) * upper).astype(jnp.bfloat16)
    result = jnp.dot(hidden, down_local, preferred_element_type=jnp.float32)
    return result.reshape(lead_shape + (down_local.shape[1],))


def body(
    resid_in,
    query_proj,
    key_proj,
    value_proj,
    query_gain,
    key_gain,
    out_weight,
    norm_gain,
    gate_weight,
    up_weight,
    down_weight,
    expert_ids,
    route_weight,
):
    tok_count = query_proj.shape[0]
    head_local = query_gain.shape[0]
    kv_local = key_gain.shape[0]
    group_size = head_local // kv_local
    positions = lax.axis_index("sp") * tok_count + lax.iota(jnp.int32, tok_count)
    cosine, sine_table = rotary_tables(positions)
    query_rot = prepare(query_proj, query_gain, cosine, sine_table)
    grouped = query_rot.reshape(tok_count, kv_local, group_size, HEAD_DIM)
    key_rot = prepare(key_proj, key_gain, cosine, sine_table).reshape(
        tok_count, kv_local * HEAD_DIM
    )
    score_factor = HEAD_DIM ** (-0.5)

    def attend_piece(running, segment):
        best_now, sums_now, accum_now = running
        seg_count = segment[0].shape[0]
        seg_keys = segment[0].reshape(seg_count, kv_local, HEAD_DIM)
        seg_values = segment[1].reshape(seg_count, kv_local, HEAD_DIM)
        scores = (
            jnp.einsum("qkgd,skd->qkgs", grouped, seg_keys, preferred_element_type=jnp.float32)
            * score_factor
        )
        new_best = jnp.maximum(best_now, jnp.max(scores, axis=-1))
        shrink = jnp.exp(best_now - new_best)
        exponents = jnp.exp(scores - new_best[..., None])
        sums_now = sums_now * shrink + jnp.sum(exponents, axis=-1)
        weights = exponents.astype(jnp.bfloat16)
        accum_now = accum_now * shrink[..., None] + jnp.einsum(
            "qkgs,skd->qkgd", weights, seg_values, preferred_element_type=jnp.float32
        )
        return (new_best, sums_now, accum_now)

    initial = (
        jnp.full((tok_count, kv_local, group_size), -jnp.inf, jnp.float32),
        jnp.zeros((tok_count, kv_local, group_size), jnp.float32),
        jnp.zeros((tok_count, kv_local, group_size, HEAD_DIM), jnp.float32),
    )
    running = initial
    segment = side_by_side((key_rot, value_proj), "sp", 0, 1)
    seg_count = segment[0].shape[0]
    sub_blocks = (
        segment[0].reshape(seg_count // 2048, 2048, segment[0].shape[1]),
        segment[1].reshape(seg_count // 2048, 2048, segment[1].shape[1]),
    )

    def scan_step(state_now, sub_block):
        return (attend_piece(state_now, sub_block), None)

    running, unused = lax.scan(scan_step, running, sub_blocks)
    best_all, sums_all, accum_all = running
    attended = (
        (accum_all / sums_all[..., None])
        .astype(jnp.bfloat16)
        .reshape(tok_count, head_local * HEAD_DIM)
    )
    tp_count = lax.axis_size("tp")
    row_count = tok_count // tp_count
    regrouped = lax.all_to_all(attended, "tp", split_axis=0, concat_axis=1, tiled=True)
    mixed_out = jnp.dot(regrouped, out_weight, preferred_element_type=jnp.float32)
    residual = (resid_in.astype(jnp.float32) + mixed_out).astype(jnp.bfloat16)
    resid_f = residual.astype(jnp.float32)
    normed = (
        resid_f * lax.rsqrt(jnp.mean(resid_f * resid_f, axis=-1, keepdims=True) + eps) * norm_gain
    ).astype(jnp.bfloat16)
    expert_count = lax.axis_size("sp")
    capacity = max(2, 3 * TOPK * TOK_DEV // (2 * tp_count * expert_count))
    own_ids = lax.dynamic_slice_in_dim(expert_ids, lax.axis_index("tp") * row_count, row_count, 0)
    slot_ids = slot_index(own_ids, expert_count, capacity)
    gate_local = gate_weight[0]
    up_local = up_weight[0]
    down_local = down_weight[0]
    outgoing = build_send(normed, own_ids, expert_count, capacity)
    received = lax.all_to_all(outgoing, "sp", split_axis=0, concat_axis=0, tiled=True)

    def expert_rows(segment, begin_row):
        return expert_ffn(segment, gate_local, up_local, down_local)

    partial_value = work_in_pieces(received[None], "tp", 0, expert_rows, 0)
    summed = summed_on_arrival(partial_value.astype(jnp.bfloat16), "tp", 0)
    expert_out = summed[0].astype(jnp.bfloat16)
    returned = lax.all_to_all(expert_out, "sp", split_axis=0, concat_axis=0, tiled=True)
    flat_out = returned.reshape(expert_count * capacity, returned.shape[-1])
    picked = (
        jnp.take(flat_out, slot_ids, axis=0)
        .astype(jnp.float32)
        .reshape(row_count, route_weight.shape[1], flat_out.shape[1])
    )
    combined = jnp.sum(picked * route_weight[:, :, None], axis=1)
    return (resid_f + combined).astype(jnp.bfloat16)


def solution(mesh):
    placed = (
        P(("sp", "tp"), None),
        P("sp", "tp"),
        P("sp", "tp"),
        P("sp", "tp"),
        P("tp", None),
        P("tp", None),
        P(),
        P(),
        P("sp", None, "tp"),
        P("sp", None, "tp"),
        P("sp", "tp", None),
        P("sp", None),
        P(("sp", "tp"), None),
    )
    return jax.shard_map(
        body, mesh=mesh, in_specs=placed, out_specs=P(("sp", "tp"), None), check_vma=False
    )
```

profile of v0, /device:TPU:1, one launch (start us, length us, event | category | flops | bytes accessed | tf_op | source)
XLA Modules:
  0.0 368.3 jit_solution(8884418520707094888)
XLA Ops:
  6.6 0.9 fusion.31
  7.5 0.8 fusion.33
  8.6 1.4 pad_maximum_fusion
  10.0 0.9 copy.60
  11.0 0.8 broadcast_multiply_fusion.2
  12.4 0.8 multiply_multiply_fusion
  13.4 77.1 %all-gather.4.cloned.1.call-done = bf16[16384,128]{0,1:T(8,128)(2,1)} async-done(((bf16[256,128]{0,1:T(8,128)(2,1)}), bf16[16384,128]{0,1:T(8,128)(2,1)}) %all-gather.4.cloned.1.call-update) | async-done | bytes 4194320 | tf_op jit(solution)/shard_map/all_gather | solution.py:18
  90.5 2.6 fusion.52
  93.1 1.6 copy.93
  94.7 1.6 copy.94
  96.2 63.1 %while.15 = (s32[]{:T(128)}, f32[256,1,2]{0,2,1:T(2,128)S(1)}, f32[256,1,2]{0,2,1:T(2,128)S(1)}, f32[256,1,2,64]{0,3,2,1:T(8,128)S(1)}, bf16[8,2048,64]{1,2,0:T(...) while((s32[]{:T(128)}, f32[256,1,2]{0,2,1:T(2,128)S(1)}, ...), condition=%wide.region_5.6_spmd.clone, body=%wide.region_2.5_spmd.clone.sunk | while | flops 276925440 | bytes 30246020 | solution.py:175
  96.2 3.7 bitcast_reduce_fusion.3
  99.9 3.2 fusion.67
  103.2 0.3 copy-done.1
  103.4 0.7 fusion.66
  104.2 3.6 bitcast_reduce_fusion.3
  107.8 3.2 fusion.67
  111.3 0.7 fusion.66
  112.1 3.6 bitcast_reduce_fusion.3
  115.7 3.2 fusion.67
  118.9 0.3 copy-done.1
  119.2 0.7 fusion.66
  119.9 3.6 bitcast_reduce_fusion.3
  123.6 3.2 fusion.67
  127.1 0.7 fusion.66
  127.8 3.6 bitcast_reduce_fusion.3
  131.5 3.2 fusion.67
  135.0 0.7 fusion.66
  135.7 3.6 bitcast_reduce_fusion.3
  139.4 3.2 fusion.67
  142.9 0.7 fusion.66
  143.6 3.6 bitcast_reduce_fusion.3
  147.3 3.2 fusion.67
  150.8 0.7 fusion.66
  151.5 3.6 bitcast_reduce_fusion.3
  155.1 3.2 fusion.67
  158.7 0.7 fusion.66
  159.6 0.7 copy.79
  160.3 4.0 %all-to-all-start = ((bf16[4,64,128]{2,1,0:T(8,128)(2,1)}), bf16[4,64,128]{2,1,0:T(8,128)(2,1)S(1)}, u32[]{:S(2)}, u32[]{:S(2)}) async-start(bf16[4,64,128]{2,1,0:T(8,128)(2,1)} %copy.79), calls=%async_computation | async-start | bytes 131072 | tf_op jit(solution)/shard_map/all_to_all | solution.py:184
  164.3 4.5 %all-to-all-done = bf16[4,64,128]{2,1,0:T(8,128)(2,1)S(1)} async-done(((bf16[4,64,128]{2,1,0:T(8,128)(2,1)}), bf16[4,64,128]{2,1,0:T(8,128)(2,1)S(1)}, u32[]{:S(2)}, u32[]{:S(2)}) %all-to-all-start) | async-done | bytes 65568 | tf_op jit(solution)/shard_map/all_to_all | solution.py:184
  168.7 0.6 multiply_reduce_fusion.1
  169.5 0.3 broadcast_in_dim.21
  169.8 1.0 reshape.392
  170.8 1.4 convolution_convert_fusion.1
  172.2 1.3 reshape.393
  173.5 37.9 %all_to_all.34 = bf16[64,3,2048]{2,1,0:T(4,128)(2,1)S(1)} all-to-all(bf16[64,3,2048]{2,1,0:T(4,128)(2,1)} %reshape.393), channel_id=1, replica_groups=mesh['sp'=64,'tp'=4] {'sp'}, dimensions={0} | all-to-all | bytes 1572864 | tf_op jit(solution)/shard_map/all_to_all | solution.py:199
  211.4 1.5 copy.68
  212.9 37.1 %all-gather.6.cloned.1.call-done = bf16[256,3,2048]{2,0,1:T(8,128)(2,1)} async-done(((bf16[64,3,2048]{2,0,1:T(8,128)(2,1)}), bf16[256,3,2048]{2,0,1:T(8,128)(2,1)}) %all-gather.6.cloned.1.call-update) | async-done | bytes 3145744 | tf_op jit(solution)/shard_map/all_gather | solution.py:38
  249.9 6.5 %copy.69 = bf16[256,3,2048]{2,1,0:T(4,128)(2,1)} copy(bf16[256,3,2048]{2,0,1:T(8,128)(2,1)} %all-gather.6.cloned.1.call-done) | data formatting | bytes 6291456 | tf_op jit(solution)/shard_map/all_gather | solution.py:38
  256.5 8.8 %reshape.394 = bf16[4,192,2048]{2,1,0:T(8,128)(2,1)} reshape(bf16[256,3,2048]{2,1,0:T(4,128)(2,1)} %copy.69) | data formatting | bytes 6291456 | tf_op jit(solution)/shard_map/vmap()/reshape | solution.py:104
  265.3 3.3 fusion.28
  268.7 1.0 fusion.25
  269.7 0.3 copy.70
  270.0 1.0 fusion.22
  271.0 39.2 %all_to_all.35 = bf16[4,1,64,3,2048]{4,2,3,1,0:T(8,128)(2,1)S(1)} all-to-all(bf16[4,1,64,3,2048]{4,2,3,1,0:T(8,128)(2,1)S(1)} %fusion.22), channel_id=1, replica_groups=mesh['sp'=64,'tp'=4] {'tp'}, dimensions={0} | all-to-all | bytes 6291456 | tf_op jit(solution)/shard_map/all_to_all | solution.py:49
  310.3 0.6 bitcast_reduce_fusion.1
  310.9 1.7 copy.74
  312.6 12.2 %all-to-all-start.3 = ((bf16[64,3,2048]{2,1,0:T(4,128)(2,1)}), bf16[64,3,2048]{2,1,0:T(4,128)(2,1)}, u32[]{:S(2)}, u32[]{:S(2)}) async-start(bf16[64,3,2048]{2,1,0:T(4,128)(2,1)} %copy.74), calls=%async_computation.3 | async-start | bytes 2097152 | tf_op jit(solution)/shard_map/all_to_all | solution.py:207
  325.5 27.4 %all-to-all-done.3 = bf16[64,3,2048]{2,1,0:T(4,128)(2,1)} async-done(((bf16[64,3,2048]{2,1,0:T(4,128)(2,1)}), bf16[64,3,2048]{2,1,0:T(4,128)(2,1)}, u32[]{:S(2)}, u32[]{:S(2)}) %all-to-all-start.3) | async-done | bytes 786464 | tf_op jit(solution)/shard_map/all_to_all | solution.py:207
  352.8 2.4 reshape.396
  355.3 1.7 gather_fusion
  357.0 1.4 gather.7
  358.4 2.3 multiply_reduce_fusion
  360.7 0.8 add_convert_fusion
  (88 shorter events, 4.0 us)
Async XLA Ops:
  6.5 162.2 %copy-start = (bf16[512,2048]{1,0:T(8,128)(2,1)S(1)}, bf16[512,2048]{1,0:T(8,128)(2,1)}, u32[]{:S(2)}) copy-start(bf16[512,2048]{1,0:T(8,128)(2,1)} %param.21) | copy-start | bytes 6291460
  6.5 83.9 %all-gather.4.cloned.1.call-start = ((), (), s32[]{:S(2)}) async-start(), calls=%async_computation.4 | async-start | bytes 4259840 | tf_op jit(solution)/shard_map/all_gather | solution.py:18
  96.2 72.5 %copy-start.4 = (bf16[64,2048]{1,0:T(8,128)(2,1)S(1)}, bf16[64,2048]{1,0:T(8,128)(2,1)}, u32[]{:S(2)}) copy-start(bf16[64,2048]{1,0:T(8,128)(2,1)} %param.15) | copy-start | bytes 786436
  99.9 3.5 copy-start.1
  107.8 3.5 copy-start.1
  115.7 3.5 copy-start.1
  123.6 3.5 copy-start.1
  131.5 3.5 copy-start.1
  139.4 3.5 copy-start.1
  147.2 3.5 copy-start.1
  155.1 3.5 copy-start.1
  159.4 9.9 %copy-start.5 = (f32[2048]{0:T(1024)S(1)}, f32[2048]{0:T(1024)}, u32[]{:S(2)}) copy-start(f32[2048]{0:T(1024)} %param.22) | copy-start | bytes 24580
  160.3 8.4 %all-to-all-start = ((bf16[4,64,128]{2,1,0:T(8,128)(2,1)}), bf16[4,64,128]{2,1,0:T(8,128)(2,1)S(1)}, u32[]{:S(2)}, u32[]{:S(2)}) async-start(bf16[4,64,128]{2,1,0:T(8,128)(2,1)} %copy.79), calls=%async_computation | async-start | bytes 131072 | tf_op jit(solution)/shard_map/all_to_all | solution.py:184
  164.3 85.7 %all-gather.6.cloned.1.call-start = ((), (), s32[]{:S(2)}) async-start(), calls=%async_computation.5 | async-start | bytes 3932160 | tf_op jit(solution)/shard_map/all_gather | solution.py:38
  265.3 3.3 copy-start.2
  265.3 3.4 copy-start.7
  268.7 1.3 copy-start.3
  310.3 15.1 %copy-start.6 = (f32[64,2]{0,1:T(2,128)S(1)}, f32[64,2]{0,1:T(2,128)}, u32[]{:S(2)}) copy-start(f32[64,2]{0,1:T(2,128)} %param.27) | copy-start | bytes 1540
  312.6 40.3 %all-to-all-start.3 = ((bf16[64,3,2048]{2,1,0:T(4,128)(2,1)}), bf16[64,3,2048]{2,1,0:T(4,128)(2,1)}, u32[]{:S(2)}, u32[]{:S(2)}) async-start(bf16[64,3,2048]{2,1,0:T(4,128)(2,1)} %copy.74), calls=%async_computation.3 | async-start | bytes 2097152 | tf_op jit(solution)/shard_map/all_to_all | solution.py:207
Sparse Core Ops, SparseCore 0:
  10.1 80.3 all-gather.3
  213.0 36.8 all-gather.5
where the time goes:
time: 369 us; the launch traced here: 368 us
  waiting for transfers between devices  146 us (40%)
  blocking collectives  77.2 us (21%)
  matrix products  62.2 us (17%)
  local copies, waits for them, and re-layouts  37.6 us (10%)
  starting transfers between devices  16.2 us (4%)
  other arithmetic  15.2 us (4%)
  between operations  13.7 us (4%)
    all_gather x1, waiting for transfers between devices, side_by_side(): lax.all_gather(both, axis, axis=dim, tiled=True)  77.1 us
    all_to_all x1, blocking collectives, summed_on_arrival(): lax.all_to_all(in_blocks(value, dim, devices), axis, 0, 0, tiled=True)  39.2 us
    all_to_all x1, blocking collectives, body(): lax.all_to_all(outgoing, 'sp', split_axis=0, concat_axis=0, tiled=True)  37.9 us
    all_gather x1, waiting for transfers between devices, work_in_pieces(): gathered.append(jax.vmap(apply)(lax.all_gather(piece, axis), starts))  37.1 us
    dot_general x8, matrix products, attend_piece(): jnp.einsum('qkgd,skd->qkgs', grouped, seg_keys, preferred_element_type=jn...  29 us
    all_to_all x1, waiting for transfers between devices, body(): lax.all_to_all(expert_out, 'sp', split_axis=0, concat_axis=0, tiled=True)  27.4 us
    dot_general x8, matrix products, attend_piece(): jnp.einsum('qkgs,skd->qkgd', weights, seg_values, preferred_element_type=...  25.9 us
    all_to_all x1, starting transfers between devices, body(): lax.all_to_all(expert_out, 'sp', split_axis=0, concat_axis=0, tiled=True)  12.2 us
  transfers between devices with their start and end apart: 4, of which 4 were waited for; matrix products, arithmetic and copies ran while one was open for 1% of the time, Pallas kernels for 0%

commit v1 on v0

--- a/solution.py
+++ b/solution.py
@@ -1,6 +1,10 @@
+import functools
+
 import jax
 import jax.numpy as jnp
 from jax import lax
+from jax.experimental import pallas as pl
+from jax.experimental.pallas import tpu as pltpu
 from jax.sharding import PartitionSpec as P
 
 HEAD_DIM = 64
@@ -11,15 +15,6 @@
 
 eps = 1e-06
 rope_base = 10000.0
-
-
-def side_by_side(arrays, axis, dim, along):
-    both = jnp.concatenate(arrays, axis=along)
-    filled, at, gathered = (lax.all_gather(both, axis, axis=dim, tiled=True), 0, [])
-    for a in arrays:
-        gathered.append(lax.slice_in_dim(filled, at, at + a.shape[along], axis=along))
-        at += a.shape[along]
-    return tuple(gathered)
 
 
 def joined_along(tiles, dim):
@@ -107,6 +102,176 @@
     hidden = (jax.nn.silu(gate) * upper).astype(jnp.bfloat16)
     result = jnp.dot(hidden, down_local, preferred_element_type=jnp.float32)
     return result.reshape(lead_shape + (down_local.shape[1],))
+
+
+LANES = 128
+MESH = pl.DeviceIdType.MESH
+LOG2E = 1.4426950408889634
+
+
+def attention_kernel(
+    q_ref, kv_ref, out_ref,
+    qall, kvall, kk, vt, osend, mlsend, orecv, mlrecv, own_o, own_ml, attv,
+    qs, qr, ks, kr, os_, or_, ms, mr, xs, xr,
+):
+    sp = lax.axis_index("sp")
+    me_x = lax.axis_index("tp")
+    z, j = sp // 8, sp % 8
+    tok = q_ref.shape[0]
+
+    def group(d):
+        return z * 8 + lax.rem(j + d, 8)
+
+    def ring(d):
+        return lax.rem(z + d, 8) * 8 + j
+
+    barrier = pltpu.get_barrier_semaphore()
+    for d in range(1, 8):
+        pl.semaphore_signal(barrier, inc=1, device_id=(group(d), me_x), device_id_type=MESH)
+        pl.semaphore_signal(barrier, inc=1, device_id=(ring(d), me_x), device_id_type=MESH)
+    for d in range(1, 4):
+        pl.semaphore_signal(barrier, inc=1, device_id=(sp, lax.rem(me_x + d, 4)), device_id_type=MESH)
+    pl.semaphore_wait(barrier, 17)
+
+    def q_copy(d):
+        return pltpu.make_async_remote_copy(
+            src_ref=q_ref, dst_ref=qall.at[d], send_sem=qs.at[d], recv_sem=qr.at[d],
+            device_id=(group(d), me_x), device_id_type=MESH)
+
+    def kv_copy(d):
+        return pltpu.make_async_remote_copy(
+            src_ref=kv_ref, dst_ref=kvall.at[d], send_sem=ks.at[d], recv_sem=kr.at[d],
+            device_id=(ring(d), me_x), device_id_type=MESH)
+
+    order = (4, 3, 5, 2, 6, 1, 7)
+    for d in order:
+        q_copy(d).start()
+        kv_copy(d).start()
+
+    lane = lax.broadcasted_iota(jnp.int32, (tok, LANES), 1)
+    low = lane < HEAD_DIM
+
+    def spread(block, at):
+        f = block.astype(jnp.float32)
+        kk[pl.ds(at * tok, tok), :] = jnp.where(low, f, pltpu.roll(f, HEAD_DIM, 1)).astype(jnp.bfloat16)
+        t = f.T.astype(jnp.bfloat16)
+        vt[0:HEAD_DIM, at * tok:(at + 1) * tok] = t[HEAD_DIM:, :]
+
+    vt[HEAD_DIM:, :] = jnp.ones((16, vt.shape[1]), jnp.bfloat16)
+    qall[0] = q_ref[...]
+    spread(kv_ref[...], 0)
+    for d in (1, 7, 2, 6, 3, 5, 4):
+        kv_copy(d).wait()
+        spread(kvall[d], d)
+    for d in range(1, 8):
+        q_copy(d).wait()
+
+    chunk = 512
+    factor = LOG2E * HEAD_DIM ** (-0.5)
+
+    def o_copy(d):
+        return pltpu.make_async_remote_copy(
+            src_ref=osend.at[d], dst_ref=orecv.at[d], send_sem=os_.at[d], recv_sem=or_.at[d],
+            device_id=(group(8 - d), me_x), device_id_type=MESH)
+
+    def ml_copy(d):
+        return pltpu.make_async_remote_copy(
+            src_ref=mlsend.at[d], dst_ref=mlrecv.at[d], send_sem=ms.at[d], recv_sem=mr.at[d],
+            device_id=(group(8 - d), me_x), device_id_type=MESH)
+
+    def block_of(q):
+        zero = jnp.zeros_like(q)
+        both = jnp.concatenate([jnp.where(low, q, zero), jnp.where(low, zero, q)], axis=0)
+        best = acc = None
+        for c in range(8 * tok // chunk):
+            keys = kk[c * chunk:(c + 1) * chunk, :]
+            s = lax.dot_general(keys, both, (((1,), (1,)), ((), ())), preferred_element_type=jnp.float32)
+            top = jnp.max(s, axis=0, keepdims=True)
+            new = top if best is None else jnp.maximum(best, top)
+            p = jnp.exp2((s - new) * factor).astype(jnp.bfloat16)
+            part = jnp.dot(vt[:, c * chunk:(c + 1) * chunk], p, preferred_element_type=jnp.float32)
+            acc = part if best is None else acc * jnp.exp2((best - new) * factor) + part
+            best = new
+        return best, acc
+
+    def put(o_ref, ml_ref, best, acc):
+        o_ref[0:HEAD_DIM, :] = acc[0:HEAD_DIM, 0:tok].astype(o_ref.dtype)
+        o_ref[HEAD_DIM:, :] = acc[0:HEAD_DIM, tok:].astype(o_ref.dtype)
+        ml_ref[0:1, :] = best
+        ml_ref[1:2, :] = acc[HEAD_DIM:HEAD_DIM + 1, :]
+
+    def step(d, carry):
+        best, acc = block_of(qall[d])
+        put(osend.at[d], mlsend.at[d], best, acc)
+        o_copy(d).start()
+        ml_copy(d).start()
+        return carry
+
+    lax.fori_loop(1, 8, step, 0)
+    best, acc = block_of(qall[0])
+    put(own_o, own_ml, best, acc)
+
+    def finish(d, carry):
+        ml_copy(d).wait()
+        o_copy(d).wait()
+        return carry
+
+    lax.fori_loop(1, 8, finish, 0)
+    tops = [own_ml[0:1, :]] + [mlrecv[d, 0:1, :] for d in range(1, 8)]
+    top = functools.reduce(jnp.maximum, tops)
+    sums = jnp.zeros_like(top)
+    heads = [jnp.zeros((HEAD_DIM, tok), jnp.float32) for _ in range(2)]
+    for d in range(8):
+        w = jnp.exp2((tops[d] - top) * factor)
+        sums = sums + w * (own_ml[1:2, :] if d == 0 else mlrecv[d, 1:2, :])
+        o = own_o[...] if d == 0 else orecv[d].astype(jnp.float32)
+        for h in range(2):
+            heads[h] = heads[h] + o[h * HEAD_DIM:(h + 1) * HEAD_DIM, :] * w[:, h * tok:(h + 1) * tok]
+    full = jnp.concatenate([heads[h] / sums[:, h * tok:(h + 1) * tok] for h in range(2)], axis=0)
+    rows = full.T.astype(jnp.bfloat16)
+    own_rows = tok // 4
+    for x in range(4):
+        attv[x] = rows[x * own_rows:(x + 1) * own_rows, :]
+
+    def x_copy(d):
+        return pltpu.make_async_remote_copy(
+            src_ref=attv.at[lax.rem(me_x + d, 4)], dst_ref=out_ref.at[me_x],
+            send_sem=xs.at[d], recv_sem=xr.at[d],
+            device_id=(sp, lax.rem(me_x + d, 4)), device_id_type=MESH)
+
+    for d in (2, 1, 3):
+        x_copy(d).start()
+    out_ref[me_x] = attv[me_x]
+    for d in (1, 3, 2):
+        x_copy(d).wait()
+
+
+def attention(q, kv):
+    tok = q.shape[0]
+    bf, f32 = jnp.bfloat16, jnp.float32
+    dma = pltpu.SemaphoreType.DMA
+    return pl.pallas_call(
+        attention_kernel,
+        out_shape=jax.ShapeDtypeStruct((4, tok // 4, LANES), bf),
+        in_specs=[pl.BlockSpec(memory_space=pltpu.VMEM)] * 2,
+        out_specs=pl.BlockSpec(memory_space=pltpu.VMEM),
+        scratch_shapes=[
+            pltpu.VMEM((8, tok, LANES), bf),
+            pltpu.VMEM((8, tok, LANES), bf),
+            pltpu.VMEM((8 * tok, LANES), bf),
+            pltpu.VMEM((HEAD_DIM + 16, 8 * tok), bf),
+            pltpu.VMEM((8, LANES, tok), bf),
+            pltpu.VMEM((8, 2, 2 * tok), f32),
+            pltpu.VMEM((8, LANES, tok), bf),
+            pltpu.VMEM((8, 2, 2 * tok), f32),
+            pltpu.VMEM((LANES, tok), f32),
+            pltpu.VMEM((2, 2 * tok), f32),
+            pltpu.VMEM((4, tok // 4, LANES), bf),
+        ] + [dma((8,))] * 8 + [dma((4,))] * 2,
+        compiler_params=pltpu.CompilerParams(
+            collective_id=0, has_side_effects=True, vmem_limit_bytes=48 << 20),
+        cost_estimate=pl.CostEstimate(flops=4 * 8 * tok * 8 * tok * 2 * HEAD_DIM, bytes_accessed=1 << 20, transcendentals=0),
+    )(q, kv)
 
 
 def body(
@@ -126,63 +291,20 @@
 ):
     tok_count = query_proj.shape[0]
     head_local = query_gain.shape[0]
-    kv_local = key_gain.shape[0]
-    group_size = head_local // kv_local
     positions = lax.axis_index("sp") * tok_count + lax.iota(jnp.int32, tok_count)
     cosine, sine_table = rotary_tables(positions)
     query_rot = prepare(query_proj, query_gain, cosine, sine_table)
-    grouped = query_rot.reshape(tok_count, kv_local, group_size, HEAD_DIM)
-    key_rot = prepare(key_proj, key_gain, cosine, sine_table).reshape(
-        tok_count, kv_local * HEAD_DIM
-    )
-    score_factor = HEAD_DIM ** (-0.5)
-
-    def attend_piece(running, segment):
-        best_now, sums_now, accum_now = running
-        seg_count = segment[0].shape[0]
-        seg_keys = segment[0].reshape(seg_count, kv_local, HEAD_DIM)
-        seg_values = segment[1].reshape(seg_count, kv_local, HEAD_DIM)
-        scores = (
-            jnp.einsum("qkgd,skd->qkgs", grouped, seg_keys, preferred_element_type=jnp.float32)
-            * score_factor
-        )
-        new_best = jnp.maximum(best_now, jnp.max(scores, axis=-1))
-        shrink = jnp.exp(best_now - new_best)
-        exponents = jnp.exp(scores - new_best[..., None])
-        sums_now = sums_now * shrink + jnp.sum(exponents, axis=-1)
-        weights = exponents.astype(jnp.bfloat16)
-        accum_now = accum_now * shrink[..., None] + jnp.einsum(
-            "qkgs,skd->qkgd", weights, seg_values, preferred_element_type=jnp.float32
-        )
-        return (new_best, sums_now, accum_now)
-
-    initial = (
-        jnp.full((tok_count, kv_local, group_size), -jnp.inf, jnp.float32),
-        jnp.zeros((tok_count, kv_local, group_size), jnp.float32),
-        jnp.zeros((tok_count, kv_local, group_size, HEAD_DIM), jnp.float32),
-    )
-    running = initial
-    segment = side_by_side((key_rot, value_proj), "sp", 0, 1)
-    seg_count = segment[0].shape[0]
-    sub_blocks = (
-        segment[0].reshape(seg_count // 2048, 2048, segment[0].shape[1]),
-        segment[1].reshape(seg_count // 2048, 2048, segment[1].shape[1]),
-    )
-
-    def scan_step(state_now, sub_block):
-        return (attend_piece(state_now, sub_block), None)
-
-    running, unused = lax.scan(scan_step, running, sub_blocks)
-    best_all, sums_all, accum_all = running
-    attended = (
-        (accum_all / sums_all[..., None])
-        .astype(jnp.bfloat16)
-        .reshape(tok_count, head_local * HEAD_DIM)
+    key_rot = prepare(key_proj, key_gain, cosine, sine_table)
+    regrouped = attention(
+        query_rot.reshape(tok_count, head_local * HEAD_DIM),
+        jnp.concatenate([key_rot.reshape(tok_count, HEAD_DIM), value_proj], axis=1),
     )
     tp_count = lax.axis_size("tp")
     row_count = tok_count // tp_count
-    regrouped = lax.all_to_all(attended, "tp", split_axis=0, concat_axis=1, tiled=True)
-    mixed_out = jnp.dot(regrouped, out_weight, preferred_element_type=jnp.float32)
+    mixed_out = jnp.einsum(
+        "xtd,xdo->to", regrouped, out_weight.reshape(tp_count, -1, out_weight.shape[1]),
+        preferred_element_type=jnp.float32,
+    )
     residual = (resid_in.astype(jnp.float32) + mixed_out).astype(jnp.bfloat16)
     resid_f = residual.astype(jnp.float32)
     normed = (

time: 369 us -> 258 us (0.70)
  waiting for transfers between devices: 146 us -> 64.6 us
  matrix products: 62.2 us -> 7.28 us
  Pallas kernels: 0 us -> 45 us
  other arithmetic: 15.2 us -> 6.97 us
  local copies, waits for them, and re-layouts: 37.6 us -> 31.1 us
  starting transfers between devices: 16.2 us -> 12.2 us
    all_gather x1 -> x0, waiting for transfers between devices: 77.1 us -> none  [side_by_side(): lax.all_gather(both, axis, axis=dim, tiled=True)]
    dot_general x17 -> x1, matrix products: 55.5 us -> 0.59 us  [body(): jnp.einsum('xtd,xdo->to', regrouped, out_weight.reshape(tp_count, -1, out...]
    pallas_call x0 -> x1, Pallas kernels: none -> 45 us  [attention(): pl.pallas_call(attention_kernel, out_shape=jax.ShapeDtypeStruct((4, tok /...]
    reduce_sum x8 -> x0, other arithmetic: 5.58 us -> none  [attend_piece(): sums_now = sums_now * shrink + jnp.sum(exponents, axis=-1)]
    all_to_all x1 -> x0, waiting for transfers between devices: 4.47 us -> none  [body(): lax.all_to_all(attended, 'tp', split_axis=0, concat_axis=1, tiled=True)]
    reshape x3 -> x0, local copies, waits for them, and re-layouts: 4.1 us -> none  [the longest x1 1.6 us: body(): segment[1].reshape(seg_count // 2048, 2048, segment[1].shape[1])]
    all_to_all x1 -> x0, starting transfers between devices: 3.96 us -> none  [body(): lax.all_to_all(attended, 'tp', split_axis=0, concat_axis=1, tiled=True)]
  transfers between devices with their start and end apart: 4 -> 2, of which waited for: 4 -> 2; matrix products, arithmetic and copies ran while one was open for 1% -> 0% of each run, Pallas kernels for 0% -> 0%
where the time goes in v1:
time: 258 us; the launch traced here: 257 us
  blocking collectives  75.9 us (29%)
  waiting for transfers between devices  64.6 us (25%)
  Pallas kernels  45 us (17%)
  local copies, waits for them, and re-layouts  31.1 us (12%)
  between operations  13.7 us (5%)
  starting transfers between devices  12.2 us (5%)
  matrix products  7.28 us (3%)
  other arithmetic  6.97 us (3%)
    pallas_call x1, Pallas kernels, attention(): pl.pallas_call(attention_kernel, out_shape=jax.ShapeDtypeStruct((4, tok /...  45 us
    all_to_all x1, blocking collectives, summed_on_arrival(): lax.all_to_all(in_blocks(value, dim, devices), axis, 0, 0, tiled=True)  39.2 us
    all_gather x1, waiting for transfers between devices, work_in_pieces(): gathered.append(jax.vmap(apply)(lax.all_gather(piece, axis), starts))  37.3 us
    all_to_all x1, blocking collectives, body(): lax.all_to_all(outgoing, 'sp', split_axis=0, concat_axis=0, tiled=True)  36.6 us
    all_to_all x1, waiting for transfers between devices, body(): lax.all_to_all(expert_out, 'sp', split_axis=0, concat_axis=0, tiled=True)  27.4 us
    all_to_all x1, starting transfers between devices, body(): lax.all_to_all(expert_out, 'sp', split_axis=0, concat_axis=0, tiled=True)  12.2 us
    reshape x1, local copies, waits for them, and re-layouts, expert_ffn(): flat_rows = rows.reshape(-1, rows.shape[-1])  8.81 us
    all_gather x1, local copies, waits for them, and re-layouts, work_in_pieces(): gathered.append(jax.vmap(apply)(lax.all_gather(piece, axis), starts))  6.52 us
  transfers between devices with their start and end apart: 2, of which 2 were waited for; matrix products, arithmetic and copies ran while one was open for 0% of the time, Pallas kernels for 0%

profile of v1, /device:TPU:1, one launch (start us, length us, event | category | flops | bytes accessed | tf_op | source)
XLA Modules:
  0.0 256.7 jit_solution(14719166852341104858)
XLA Ops:
  6.5 0.0 copy-start
  6.5 0.0 all-gather.3.cloned.1.call-start
  6.6 0.1 fusion.21
  6.6 0.1 fusion.27
  6.8 0.1 copy.61
  6.9 0.1 copy.62
  7.0 1.1 copy.60
  8.0 0.1 fusion.10
  8.2 0.9 copy.64
  9.0 0.9 copy.59
  10.0 0.1 fusion.20
  10.2 0.8 fusion.14
  11.0 0.1 copy.65.q_ref
  11.1 0.8 fusion.12
  11.9 0.5 fusion.15
  12.3 0.1 pad_maximum_fusion.1.kv_ref
  12.5 0.0 copy-start.3
  12.5 0.0 copy-start.4
  12.5 45.0 %shard_map.127 = bf16[4,64,128]{2,1,0:T(8,128)(2,1)S(1)} custom-call(bf16[256,128]{1,0:T(8,128)(2,1)S(1)} %copy.65.q_ref, bf16[256,128]{1,0:T(8,128)(2,1)S(1)} %pad_maximum_fusion.1.kv_ref), custom_call_target="tpu_custom_call" | custom-call | flops 2147483648 | bytes 1048576 | tf_op jit(solution)/shard_map/pallas_call | solution.py:253
  57.5 0.0 copy-done
  57.5 0.0 copy-start.6
  57.5 0.0 copy-done.3
  57.5 0.6 multiply_reduce_fusion.1
  58.1 0.0 copy-done.4
  58.1 0.1 multiply_convert_fusion
  58.2 0.3 broadcast_in_dim.10
  58.5 1.0 reshape.321
  59.5 0.0 copy-done.6
  59.5 0.1 broadcast_multiply_fusion.2
  59.6 0.1 copy.66
  59.7 0.1 reshape.320
  59.8 0.1 fusion.17
  59.9 0.2 reduce_window_sum.12
  60.1 0.2 select_reduce_fusion
  60.3 1.4 convolution_convert_fusion.1
  61.7 1.3 reshape.322
  63.0 36.6 %all_to_all.15 = bf16[64,3,2048]{2,1,0:T(4,128)(2,1)S(1)} all-to-all(bf16[64,3,2048]{2,1,0:T(4,128)(2,1)} %reshape.322), channel_id=1, replica_groups=mesh['sp'=64,'tp'=4] {'sp'}, dimensions={0} | all-to-all | bytes 1572864 | tf_op jit(solution)/shard_map/all_to_all | solution.py:321
  99.6 1.5 copy.69
  101.1 0.0 all-gather.3.cloned.1.call-update
  101.1 37.3 %all-gather.3.cloned.1.call-done = bf16[256,3,2048]{2,0,1:T(8,128)(2,1)} async-done(((bf16[64,3,2048]{2,0,1:T(8,128)(2,1)}), bf16[256,3,2048]{2,0,1:T(8,128)(2,1)}) %all-gather.3.cloned.1.call-update) | async-done | bytes 3145744 | tf_op jit(solution)/shard_map/all_gather | solution.py:33
  138.4 6.5 %copy.70 = bf16[256,3,2048]{2,1,0:T(4,128)(2,1)} copy(bf16[256,3,2048]{2,0,1:T(8,128)(2,1)} %all-gather.3.cloned.1.call-done) | data formatting | bytes 6291456 | tf_op jit(solution)/shard_map/all_gather | solution.py:33
  144.9 8.8 %reshape.323 = bf16[4,192,2048]{2,1,0:T(8,128)(2,1)} reshape(bf16[256,3,2048]{2,1,0:T(4,128)(2,1)} %copy.70) | data formatting | bytes 6291456 | tf_op jit(solution)/shard_map/vmap()/reshape | solution.py:99
  153.7 3.3 %fusion.7 = f32[4,192,256]{2,1,0:T(8,128)S(1)} fusion(bf16[4,192,2048]{2,1,0:T(8,128)(2,1)} %reshape.323, bf16[1,2048,256]{2,1,0:T(8,128)(2,1)} %param.21), kind=kOutput, calls=%fused_computation.13 | convolution fusion | flops 805306368 | bytes 4980736 | tf_op jit(solution)/shard_map/vmap()/dot_general | solution.py:100
  157.0 0.1 copy-done.7
  157.1 1.0 fusion.4
  158.1 0.3 copy.71
  158.5 1.0 fusion
  159.5 39.2 %all_to_all.16 = bf16[4,1,64,3,2048]{4,2,3,1,0:T(8,128)(2,1)S(1)} all-to-all(bf16[4,1,64,3,2048]{4,2,3,1,0:T(8,128)(2,1)S(1)} %fusion), channel_id=1, replica_groups=mesh['sp'=64,'tp'=4] {'tp'}, dimensions={0} | all-to-all | bytes 6291456 | tf_op jit(solution)/shard_map/all_to_all | solution.py:44
  198.7 0.6 bitcast_reduce_fusion
  199.3 1.7 copy.75
  201.0 12.2 %all-to-all-start.2 = ((bf16[64,3,2048]{2,1,0:T(4,128)(2,1)}), bf16[64,3,2048]{2,1,0:T(4,128)(2,1)}, u32[]{:S(2)}, u32[]{:S(2)}) async-start(bf16[64,3,2048]{2,1,0:T(4,128)(2,1)} %copy.75), calls=%async_computation.2 | async-start | bytes 2097152 | tf_op jit(solution)/shard_map/all_to_all | solution.py:329
  213.2 0.1 reduce_sum.68
  213.3 0.1 copy.76
  213.4 0.1 mul.235
  213.6 0.1 copy.67
  213.7 0.1 copy.68
  213.8 0.0 copy-done.5
  213.8 0.1 copy.77
  213.9 27.4 %all-to-all-done.2 = bf16[64,3,2048]{2,1,0:T(4,128)(2,1)} async-done(((bf16[64,3,2048]{2,1,0:T(4,128)(2,1)}), bf16[64,3,2048]{2,1,0:T(4,128)(2,1)}, u32[]{:S(2)}, u32[]{:S(2)}) %all-to-all-start.2) | async-done | bytes 786464 | tf_op jit(solution)/shard_map/all_to_all | solution.py:329
  241.3 2.4 reshape.325
  243.7 1.7 gather_fusion
  245.4 1.4 gather.7
  246.8 2.3 multiply_reduce_fusion
  249.1 0.8 add_convert_fusion
  (18 shorter events, 0.2 us)
Async XLA Ops:
  6.5 50.9 %copy-start = (bf16[512,2048]{1,0:T(8,128)(2,1)S(1)}, bf16[512,2048]{1,0:T(8,128)(2,1)}, u32[]{:S(2)}) copy-start(bf16[512,2048]{1,0:T(8,128)(2,1)} %param.19) | copy-start | bytes 6291460
  6.5 131.8 %all-gather.3.cloned.1.call-start = ((), (), s32[]{:S(2)}) async-start(), calls=%async_computation.3 | async-start | bytes 3932160 | tf_op jit(solution)/shard_map/all_gather | solution.py:33
  12.5 45.0 %copy-start.3 = (bf16[64,2048]{1,0:T(8,128)(2,1)S(1)}, bf16[64,2048]{1,0:T(8,128)(2,1)}, u32[]{:S(2)}) copy-start(bf16[64,2048]{1,0:T(8,128)(2,1)} %param.13) | copy-start | bytes 786436
  12.5 45.6 %copy-start.4 = (f32[2048]{0:T(1024)S(1)}, f32[2048]{0:T(1024)}, u32[]{:S(2)}) copy-start(f32[2048]{0:T(1024)} %param.20) | copy-start | bytes 24580
  57.5 2.1 copy-start.6
  153.7 3.3 %copy-start.1 = (bf16[4,192,2048]{2,1,0:T(8,128)(2,1)S(1)}, bf16[4,192,2048]{2,1,0:T(8,128)(2,1)}, u32[]{:S(2)}) copy-start(bf16[4,192,2048]{2,1,0:T(8,128)(2,1)} %reshape.323) | copy-start | bytes 9437188
  153.7 3.4 %copy-start.7 = (bf16[1,2048,256]{2,1,0:T(8,128)(2,1)S(1)}, bf16[1,2048,256]{2,1,0:T(8,128)(2,1)}, u32[]{:S(2)}) copy-start(bf16[1,2048,256]{2,1,0:T(8,128)(2,1)} %param.22) | copy-start | bytes 3145732
  157.1 1.3 copy-start.2
  198.7 15.1 %copy-start.5 = (f32[64,2]{0,1:T(2,128)S(1)}, f32[64,2]{0,1:T(2,128)}, u32[]{:S(2)}) copy-start(f32[64,2]{0,1:T(2,128)} %param.25) | copy-start | bytes 1540
  201.0 40.3 %all-to-all-start.2 = ((bf16[64,3,2048]{2,1,0:T(4,128)(2,1)}), bf16[64,3,2048]{2,1,0:T(4,128)(2,1)}, u32[]{:S(2)}, u32[]{:S(2)}) async-start(bf16[64,3,2048]{2,1,0:T(4,128)(2,1)} %copy.75), calls=%async_computation.2 | async-start | bytes 2097152 | tf_op jit(solution)/shard_map/all_to_all | solution.py:329
Sparse Core Ops, SparseCore 0:
  101.2 37.0 all-gather.2

commit v2 on v1

--- a/solution.py
+++ b/solution.py
@@ -15,34 +15,6 @@
 
 eps = 1e-06
 rope_base = 10000.0
-
-
-def joined_along(tiles, dim):
-    dims = list(tiles.shape[1:])
-    dims[dim] *= tiles.shape[0]
-    return jnp.moveaxis(tiles, 0, dim).reshape(dims)
-
-
-def work_in_pieces(value, axis, dim, apply, out_dim):
-    devices, width = (lax.axis_size(axis), value.shape[dim])
-    count = 2 if width % 2 == 0 else 1
-    gathered, length = ([], width // count)
-    for k in range(count):
-        piece = lax.slice_in_dim(value, k * length, (k + 1) * length, axis=dim)
-        starts = jnp.arange(devices) * width + k * length
-        gathered.append(jax.vmap(apply)(lax.all_gather(piece, axis), starts))
-    return joined_along(jnp.concatenate(gathered, axis=out_dim + 1), out_dim)
-
-
-def in_blocks(value, dim, devices):
-    before, after = (value.shape[:dim], value.shape[dim + 1 :])
-    return jnp.moveaxis(value.reshape(*before, devices, -1, *after), dim, 0)
-
-
-def summed_on_arrival(value, axis, dim):
-    devices = lax.axis_size(axis)
-    tiles = lax.all_to_all(in_blocks(value, dim, devices), axis, 0, 0, tiled=True)
-    return jnp.sum(tiles.astype(jnp.float32), axis=0)
 
 
 def rotary_tables(positions):
@@ -75,44 +47,15 @@
     return rotated.astype(jnp.bfloat16)
 
 
-def slot_index(ids_rows, expert_count, capacity):
-    flat_ids = ids_rows.reshape(-1)
-    member = (flat_ids[:, None] == jnp.arange(expert_count, dtype=jnp.int32)[None, :]).astype(
-        jnp.int32
-    )
-    ranks = jnp.sum((jnp.cumsum(member, axis=0) - member) * member, axis=1)
-    return flat_ids * capacity + ranks
-
-
-def build_send(rows, ids_rows, expert_count, capacity):
-    slot_ids = slot_index(ids_rows, expert_count, capacity)
-    picker = (
-        jnp.arange(expert_count * capacity, dtype=jnp.int32)[:, None] == slot_ids[None, :]
-    ).astype(jnp.bfloat16)
-    repeated = jnp.repeat(rows, ids_rows.shape[1], axis=0)
-    outgoing = jnp.dot(picker, repeated, preferred_element_type=jnp.float32).astype(jnp.bfloat16)
-    return outgoing.reshape(expert_count, capacity, rows.shape[1])
-
-
-def expert_ffn(rows, gate_local, up_local, down_local):
-    lead_shape = rows.shape[:-1]
-    flat_rows = rows.reshape(-1, rows.shape[-1])
-    gate = jnp.dot(flat_rows, gate_local, preferred_element_type=jnp.float32)
-    upper = jnp.dot(flat_rows, up_local, preferred_element_type=jnp.float32)
-    hidden = (jax.nn.silu(gate) * upper).astype(jnp.bfloat16)
-    result = jnp.dot(hidden, down_local, preferred_element_type=jnp.float32)
-    return result.reshape(lead_shape + (down_local.shape[1],))
-
-
 LANES = 128
 MESH = pl.DeviceIdType.MESH
 LOG2E = 1.4426950408889634
 
 
 def attention_kernel(
-    q_ref, kv_ref, out_ref,
+    q_ref, kv_ref, down_ref, out_ref, others_ref,
     qall, kvall, kk, vt, osend, mlsend, orecv, mlrecv, own_o, own_ml, attv,
-    qs, qr, ks, kr, os_, or_, ms, mr, xs, xr,
+    qs, qr, ks, kr, os_, or_, ms, mr, xs, xr, ds, dr,
 ):
     sp = lax.axis_index("sp")
     me_x = lax.axis_index("tp")
@@ -147,6 +90,25 @@
     for d in order:
         q_copy(d).start()
         kv_copy(d).start()
+
+    right, left = lax.rem(me_x + 1, 4), lax.rem(me_x + 3, 4)
+    half = down_ref.shape[0] // 2
+
+    def down_copy(way):
+        return pltpu.make_async_remote_copy(
+            src_ref=down_ref, dst_ref=others_ref.at[2 * way],
+            send_sem=ds.at[way], recv_sem=dr.at[way],
+            device_id=(sp, left if way == 0 else right), device_id_type=MESH)
+
+    def down_pass(way):
+        part = pl.ds(half * way, half)
+        return pltpu.make_async_remote_copy(
+            src_ref=others_ref.at[2 * way, part], dst_ref=others_ref.at[1, part],
+            send_sem=ds.at[2 + way], recv_sem=dr.at[2 + way],
+            device_id=(sp, left if way == 0 else right), device_id_type=MESH)
+
+    for way in range(2):
+        down_copy(way).start()
 
     lane = lax.broadcasted_iota(jnp.int32, (tok, LANES), 1)
     low = lane < HEAD_DIM
@@ -200,7 +162,13 @@
         ml_ref[0:1, :] = best
         ml_ref[1:2, :] = acc[HEAD_DIM:HEAD_DIM + 1, :]
 
+    def down_turn():
+        for way in range(2):
+            down_copy(way).wait()
+            down_pass(way).start()
+
     def step(d, carry):
+        pl.when(d == 5)(down_turn)
         best, acc = block_of(qall[d])
         put(osend.at[d], mlsend.at[d], best, acc)
         o_copy(d).start()
@@ -244,17 +212,19 @@
     out_ref[me_x] = attv[me_x]
     for d in (1, 3, 2):
         x_copy(d).wait()
-
-
-def attention(q, kv):
+    for way in range(2):
+        down_pass(way).wait()
+
+
+def attention(q, kv, down):
     tok = q.shape[0]
     bf, f32 = jnp.bfloat16, jnp.float32
     dma = pltpu.SemaphoreType.DMA
     return pl.pallas_call(
         attention_kernel,
-        out_shape=jax.ShapeDtypeStruct((4, tok // 4, LANES), bf),
-        in_specs=[pl.BlockSpec(memory_space=pltpu.VMEM)] * 2,
-        out_specs=pl.BlockSpec(memory_space=pltpu.VMEM),
+        out_shape=(jax.ShapeDtypeStruct((4, tok // 4, LANES), bf), jax.ShapeDtypeStruct((3,) + down.shape, bf)),
+        in_specs=[pl.BlockSpec(memory_space=pltpu.VMEM)] * 2 + [pl.BlockSpec(memory_space=pl.ANY)],
+        out_specs=(pl.BlockSpec(memory_space=pltpu.VMEM), pl.BlockSpec(memory_space=pl.ANY)),
         scratch_shapes=[
             pltpu.VMEM((8, tok, LANES), bf),
             pltpu.VMEM((8, tok, LANES), bf),
@@ -267,11 +237,230 @@
             pltpu.VMEM((LANES, tok), f32),
             pltpu.VMEM((2, 2 * tok), f32),
             pltpu.VMEM((4, tok // 4, LANES), bf),
-        ] + [dma((8,))] * 8 + [dma((4,))] * 2,
+        ] + [dma((8,))] * 8 + [dma((4,))] * 4,
         compiler_params=pltpu.CompilerParams(
             collective_id=0, has_side_effects=True, vmem_limit_bytes=48 << 20),
         cost_estimate=pl.CostEstimate(flops=4 * 8 * tok * 8 * tok * 2 * HEAD_DIM, bytes_accessed=1 << 20, transcendentals=0),
-    )(q, kv)
+    )(q, kv, down)
+
+
+def order_of(i):
+    return lax.rem(8 + (2 * lax.rem(i, 2) - 1) * ((i + 1) // 2), 8)
+
+
+LAGS = (1, 2, 3)
+
+
+def expert_kernel(
+    src_ref, slot_ref, route_ref, att_ref, resid_ref, outw_ref, gain_ref, gate_ref, up_ref, down_ref, others_ref,
+    out_ref,
+    dcat, res3, normed3, sendbuf, recv, xall, hall, hsend, retsend, ret, out3,
+    dsem, ss, sr, axs, axr, bxs, bxr, hs, hr, ts, tr,
+):
+    sp = lax.axis_index("sp")
+    me_x = lax.axis_index("tp")
+    z, j = sp // 8, sp % 8
+    right, left = lax.rem(me_x + 1, 4), lax.rem(me_x + 3, 4)
+
+    def peer(k):
+        return lax.rem(z + k // 8, 8) * 8 + lax.rem(j + lax.rem(k, 8), 8)
+
+    def source(k):
+        return lax.rem(z + 8 - k // 8, 8) * 8 + lax.rem(j + 8 - lax.rem(k, 8), 8)
+
+    own_down = pltpu.make_async_copy(down_ref, dcat.at[0], dsem.at[0])
+    other_down = pltpu.make_async_copy(others_ref, dcat.at[pl.ds(1, 3)], dsem.at[1])
+    own_down.start()
+    other_down.start()
+    barrier = pltpu.get_barrier_semaphore()
+
+    def greet(k, carry):
+        pl.semaphore_signal(barrier, inc=1, device_id=(peer(k), me_x), device_id_type=MESH)
+        return carry
+
+    lax.fori_loop(1, 64, greet, 0)
+    for d in range(1, 4):
+        pl.semaphore_signal(barrier, inc=1, device_id=(sp, lax.rem(me_x + d, 4)), device_id_type=MESH)
+
+    rows = resid_ref.shape[0]
+    mixed = jnp.zeros(resid_ref.shape, jnp.float32)
+    for x in range(4):
+        mixed = mixed + jnp.dot(att_ref[x], outw_ref[x * LANES:(x + 1) * LANES, :], preferred_element_type=jnp.float32)
+    residual = (resid_ref[...].astype(jnp.float32) + mixed).astype(jnp.bfloat16)
+    resid_f = residual.astype(jnp.float32)
+    scale = lax.rsqrt(jnp.mean(resid_f * resid_f, axis=-1, keepdims=True) + eps)
+    normed = (resid_f * scale * gain_ref[...]).astype(jnp.bfloat16)
+    res3[...] = residual.reshape(rows, 16, LANES)
+    normed3[...] = normed.reshape(rows, 16, LANES)
+
+    def fill(i, carry):
+        for k in range(3):
+            sendbuf[i, k] = normed3[src_ref[3 * i + k]]
+        return carry
+
+    lax.fori_loop(0, 64, fill, 0)
+    pl.semaphore_wait(barrier, 66)
+
+    def dispatch(i, carry):
+        dz = order_of(i // 8)
+        k = dz * 8 + lax.rem(i, 8)
+
+        pltpu.make_async_remote_copy(
+            src_ref=sendbuf.at[k], dst_ref=recv.at[dz, lax.rem(i, 8)], send_sem=ss, recv_sem=sr.at[dz],
+            device_id=(peer(k), me_x), device_id_type=MESH).start()
+        return carry
+
+    lax.fori_loop(1, 64, dispatch, 0)
+    recv[0, 0] = sendbuf[0]
+
+    def a_copy(dz, way):
+        return pltpu.make_async_remote_copy(
+            src_ref=recv.at[dz], dst_ref=xall.at[2 * way, dz],
+            send_sem=axs.at[way, dz], recv_sem=axr.at[way, dz],
+            device_id=(sp, left if way == 0 else right), device_id_type=MESH)
+
+    def b_copy(dz, way):
+        part = pl.ds(4 * way, 4)
+        return pltpu.make_async_remote_copy(
+            src_ref=xall.at[2 * way, dz, part], dst_ref=xall.at[1, dz, part],
+            send_sem=bxs.at[way, dz], recv_sem=bxr.at[way, dz],
+            device_id=(sp, left if way == 0 else right), device_id_type=MESH)
+
+    def h_copy(dz, d):
+        return pltpu.make_async_remote_copy(
+            src_ref=hsend.at[d, dz], dst_ref=hall.at[d, dz],
+            send_sem=hs.at[d, dz], recv_sem=hr.at[d, dz],
+            device_id=(sp, lax.rem(me_x + d, 4)), device_id_type=MESH)
+
+    def stage_a(dz):
+        @pl.when(dz == 0)
+        def _():
+            pltpu.make_async_copy(recv.at[0, pl.ds(1, 7)], recv.at[0, pl.ds(1, 7)], sr.at[0]).wait()
+
+        @pl.when(dz > 0)
+        def _():
+            pltpu.make_async_copy(recv.at[dz], recv.at[dz], sr.at[dz]).wait()
+
+        for way in range(2):
+            a_copy(dz, way).start()
+
+    def stage_b(dz):
+        for way in range(2):
+            a_copy(dz, way).wait()
+            b_copy(dz, way).start()
+
+    def stage_c(dz):
+        for way in range(2):
+            b_copy(dz, way).wait()
+        block = jnp.concatenate([recv[dz].reshape(24, 16, LANES)] + [xall[d, dz].reshape(24, 16, LANES) for d in range(3)], axis=0)
+        block = block.reshape(96, 16 * LANES)
+        gate = jnp.dot(block, gate_ref[...], preferred_element_type=jnp.float32)
+        upper = jnp.dot(block, up_ref[...], preferred_element_type=jnp.float32)
+        hidden = (gate / (1.0 + jnp.exp(-gate)) * upper).astype(jnp.bfloat16)
+        hall[0, dz] = hidden[0:24]
+        for d in range(1, 4):
+            hsend[d, dz] = hidden[24 * d:24 * (d + 1)]
+        for d in range(1, 4):
+            h_copy(d=d, dz=dz).start()
+
+    def stage_d(dz):
+        for d in range(1, 4):
+            h_copy(dz, d).wait()
+        full = jnp.dot(hall[0, dz], dcat[0], preferred_element_type=jnp.float32)
+        for d in range(1, 4):
+            full = full + jnp.dot(hall[d, dz], dcat[4 - d], preferred_element_type=jnp.float32)
+        tiles = full.astype(jnp.bfloat16).reshape(8, 3, 16, LANES)
+        retsend[dz] = tiles
+
+        @pl.when(dz == 0)
+        def _():
+            ret[0:3] = retsend[0, 0]
+
+        def give(q, carry):
+            k = dz * 8 + q
+            pltpu.make_async_remote_copy(
+                src_ref=retsend.at[dz, q], dst_ref=ret.at[pl.ds(3 * k, 3)], send_sem=ts, recv_sem=tr,
+                device_id=(source(k), me_x), device_id_type=MESH).start()
+            return carry
+
+        lax.fori_loop(1 - lax.min(dz, 1), 8, give, 0)
+
+    def wait_down():
+        own_down.wait()
+        other_down.wait()
+
+    la, lb, lc = LAGS
+
+    def step(t, carry):
+        pl.when(t < 8)(lambda: stage_a(order_of(t)))
+        pl.when((t >= la) & (t < 8 + la))(lambda: stage_b(order_of(t - la)))
+        pl.when((t >= lb) & (t < 8 + lb))(lambda: stage_c(order_of(t - lb)))
+        pl.when(t == lc)(wait_down)
+        pl.when((t >= lc) & (t < 8 + lc))(lambda: stage_d(order_of(t - lc)))
+        return carry
+
+    lax.fori_loop(0, 8 + lc, step, 0)
+    pltpu.make_async_copy(ret.at[pl.ds(3, 189)], ret.at[pl.ds(3, 189)], tr).wait()
+
+    def join(t, carry):
+        total = res3[t].astype(jnp.float32)
+        both = jnp.zeros_like(total)
+        for k in range(TOPK):
+            both = both + ret[slot_ref[TOPK * t + k]].astype(jnp.float32) * route_ref[TOPK * t + k]
+        out3[t] = (total + both).astype(jnp.bfloat16)
+        return carry
+
+    lax.fori_loop(0, rows, join, 0)
+    out_ref[...] = out3[...].reshape(rows, 16 * LANES)
+    pltpu.make_async_copy(sendbuf.at[pl.ds(1, 63)], sendbuf.at[pl.ds(1, 63)], ss).wait()
+    pltpu.make_async_copy(sendbuf.at[pl.ds(1, 63)], sendbuf.at[pl.ds(1, 63)], ts).wait()
+
+
+def experts(src, slot, route, att, resid, outw, gain, gate, up, down, others):
+    rows = resid.shape[0]
+    bf = jnp.bfloat16
+    dma = pltpu.SemaphoreType.DMA
+    smem = pl.BlockSpec(memory_space=pltpu.SMEM)
+    vmem = pl.BlockSpec(memory_space=pltpu.VMEM)
+    hbm = pl.BlockSpec(memory_space=pl.ANY)
+    return pl.pallas_call(
+        expert_kernel,
+        out_shape=jax.ShapeDtypeStruct(resid.shape, bf),
+        in_specs=[smem] * 3 + [vmem] * 6 + [hbm] * 2,
+        out_specs=vmem,
+        scratch_shapes=[
+            pltpu.VMEM((4,) + down.shape, bf),
+            pltpu.VMEM((rows, 16, LANES), bf),
+            pltpu.VMEM((rows, 16, LANES), bf),
+            pltpu.VMEM((64, 3, 16, LANES), bf),
+            pltpu.VMEM((8, 8, 3, 16, LANES), bf),
+            pltpu.VMEM((3, 8, 8, 3, 16, LANES), bf),
+            pltpu.VMEM((4, 8, 24, down.shape[0]), bf),
+            pltpu.VMEM((4, 8, 24, down.shape[0]), bf),
+            pltpu.VMEM((8, 8, 3, 16, LANES), bf),
+            pltpu.VMEM((192, 16, LANES), bf),
+            pltpu.VMEM((rows, 16, LANES), bf),
+            dma((2,)), dma(()), dma((8,)), dma((2, 8)), dma((2, 8)), dma((2, 8)), dma((2, 8)),
+            dma((4, 8)), dma((4, 8)), dma(()), dma(()),
+        ],
+        compiler_params=pltpu.CompilerParams(
+            collective_id=1, has_side_effects=True, vmem_limit_bytes=56 << 20),
+        cost_estimate=pl.CostEstimate(flops=6 * 768 * 2048 * 256, bytes_accessed=8 << 20, transcendentals=0),
+    )(src, slot, route, att, resid, outw, gain, gate, up, down, others)
+
+
+def routing(own_ids):
+    sp = lax.axis_index("sp")
+    flat = own_ids.reshape(-1)
+    count = flat.shape[0]
+    item = jnp.arange(count, dtype=jnp.int32)
+    earlier = (flat[:, None] == flat[None, :]) & (item[None, :] < item[:, None])
+    rank = jnp.sum(earlier.astype(jnp.int32), axis=1)
+    place = ((flat // 8 - sp // 8) % 8) * 8 + (flat - sp) % 8
+    slot = place * 3 + rank
+    named = jnp.arange(192, dtype=jnp.int32)[:, None] == slot[None, :]
+    src = jnp.sum(jnp.where(named, item[None, :] // TOPK, 0), axis=1)
+    return slot, src
 
 
 def body(
@@ -295,46 +484,18 @@
     cosine, sine_table = rotary_tables(positions)
     query_rot = prepare(query_proj, query_gain, cosine, sine_table)
     key_rot = prepare(key_proj, key_gain, cosine, sine_table)
-    regrouped = attention(
+    row_count = tok_count // lax.axis_size("tp")
+    own_ids = lax.dynamic_slice_in_dim(expert_ids, lax.axis_index("tp") * row_count, row_count, 0)
+    slot, src = routing(own_ids)
+    regrouped, others = attention(
         query_rot.reshape(tok_count, head_local * HEAD_DIM),
         jnp.concatenate([key_rot.reshape(tok_count, HEAD_DIM), value_proj], axis=1),
+        down_weight[0],
     )
-    tp_count = lax.axis_size("tp")
-    row_count = tok_count // tp_count
-    mixed_out = jnp.einsum(
-        "xtd,xdo->to", regrouped, out_weight.reshape(tp_count, -1, out_weight.shape[1]),
-        preferred_element_type=jnp.float32,
+    return experts(
+        src, slot, route_weight.reshape(-1), regrouped, resid_in, out_weight, norm_gain[None],
+        gate_weight[0], up_weight[0], down_weight[0], others,
     )
-    residual = (resid_in.astype(jnp.float32) + mixed_out).astype(jnp.bfloat16)
-    resid_f = residual.astype(jnp.float32)
-    normed = (
-        resid_f * lax.rsqrt(jnp.mean(resid_f * resid_f, axis=-1, keepdims=True) + eps) * norm_gain
-    ).astype(jnp.bfloat16)
-    expert_count = lax.axis_size("sp")
-    capacity = max(2, 3 * TOPK * TOK_DEV // (2 * tp_count * expert_count))
-    own_ids = lax.dynamic_slice_in_dim(expert_ids, lax.axis_index("tp") * row_count, row_count, 0)
-    slot_ids = slot_index(own_ids, expert_count, capacity)
-    gate_local = gate_weight[0]
-    up_local = up_weight[0]
-    down_local = down_weight[0]
-    outgoing = build_send(normed, own_ids, expert_count, capacity)
-    received = lax.all_to_all(outgoing, "sp", split_axis=0, concat_axis=0, tiled=True)
-
-    def expert_rows(segment, begin_row):
-        return expert_ffn(segment, gate_local, up_local, down_local)
-
-    partial_value = work_in_pieces(received[None], "tp", 0, expert_rows, 0)
-    summed = summed_on_arrival(partial_value.astype(jnp.bfloat16), "tp", 0)
-    expert_out = summed[0].astype(jnp.bfloat16)
-    returned = lax.all_to_all(expert_out, "sp", split_axis=0, concat_axis=0, tiled=True)
-    flat_out = returned.reshape(expert_count * capacity, returned.shape[-1])
-    picked = (
-        jnp.take(flat_out, slot_ids, axis=0)
-        .astype(jnp.float32)
-        .reshape(row_count, route_weight.shape[1], flat_out.shape[1])
-    )
-    combined = jnp.sum(picked * route_weight[:, :, None], axis=1)
-    return (resid_f + combined).astype(jnp.bfloat16)
 
 
 def solution(mesh):

time: 258 us -> 127 us (0.49)
  blocking collectives: 75.9 us -> 0 us
  Pallas kernels: 45 us -> 112 us
  waiting for transfers between devices: 64.6 us -> 0 us
  local copies, waits for them, and re-layouts: 31.1 us -> 10.6 us
  between operations: 13.7 us -> 0.17 us
  starting transfers between devices: 12.2 us -> 0 us
  matrix products: 7.28 us -> 0 us
  other arithmetic: 6.97 us -> 3.55 us
    all_to_all x2 -> x0, blocking collectives: 75.9 us -> none  [the longest x1 39.2 us: summed_on_arrival(): lax.all_to_all(in_blocks(value, dim, devices), axis, 0, 0, tiled=True)]
    pallas_call x1 -> x2, Pallas kernels: 45 us -> 112 us  [the longest x1 65.8 us: experts(): pl.pallas_call(expert_kernel, out_shape=jax.ShapeDtypeStruct(resid.shape,...]
    all_gather x1 -> x0, waiting for transfers between devices: 37.3 us -> none  [work_in_pieces(): gathered.append(jax.vmap(apply)(lax.all_gather(piece, axis), starts))]
    all_to_all x1 -> x0, waiting for transfers between devices: 27.4 us -> none  [body(): lax.all_to_all(expert_out, 'sp', split_axis=0, concat_axis=0, tiled=True)]
    reshape x5 -> x2, local copies, waits for them, and re-layouts: 13.6 us -> 0.79 us  [the longest x1 0.65 us: body(): route_weight.reshape(-1)]
    all_to_all x1 -> x0, starting transfers between devices: 12.2 us -> none  [body(): lax.all_to_all(expert_out, 'sp', split_axis=0, concat_axis=0, tiled=True)]
    dot_general x5 -> x0, matrix products: 7.28 us -> none  [the longest x1 3.31 us: expert_ffn(): gate = jnp.dot(flat_rows, gate_local, preferred_element_type=jnp.float32)]
    all_gather x1 -> x0, local copies, waits for them, and re-layouts: 6.52 us -> none  [work_in_pieces(): gathered.append(jax.vmap(apply)(lax.all_gather(piece, axis), starts))]
  transfers between devices with their start and end apart: 2 -> 0, of which waited for: 2 -> 0; matrix products, arithmetic and copies ran while one was open for 0% -> 0% of each run, Pallas kernels for 0% -> 0%
where the time goes in v2:
time: 127 us
  Pallas kernels  112 us (88%)
  local copies, waits for them, and re-layouts  10.6 us (8%)
  other arithmetic  3.55 us (3%)
    pallas_call x1, Pallas kernels, experts(): pl.pallas_call(expert_kernel, out_shape=jax.ShapeDtypeStruct(resid.shape,...  65.8 us
    pallas_call x1, Pallas kernels, attention(): pl.pallas_call(attention_kernel, out_shape=(jax.ShapeDtypeStruct((4, tok...  46.6 us
    unnamed x15, local copies, waits for them, and re-layouts  9.31 us

profile of v2, /device:TPU:1, one launch (start us, length us, event | category | flops | bytes accessed | tf_op | source)
XLA Modules:
  0.0 126.6 jit_solution(305119039502293466)
XLA Ops:
  0.0 0.0 copy-start
  0.0 0.7 copy-done
  0.7 0.1 constant_dynamic-slice_fusion
  0.8 0.1 copy.42
  0.9 0.1 reshape.336
  1.0 0.2 convert_reduce_fusion
  1.2 0.0 copy-start.4
  1.2 0.7 select_reduce_fusion.src_ref
  2.0 0.8 copy.43
  2.7 0.7 reshape.337.route_ref
  3.4 0.1 fusion.10
  3.4 0.1 fusion.19
  3.6 0.9 copy.44
  4.6 0.8 fusion.4
  5.3 0.9 copy.45
  6.2 0.1 fusion
  6.3 0.8 fusion.2
  7.1 0.9 copy.49
  8.0 0.1 fusion.9
  8.2 0.1 copy.50.q_ref
  8.3 0.1 copy.46
  8.4 0.1 copy.47
  8.5 0.5 fusion.5
  9.0 0.1 pad_maximum_fusion.1.kv_ref
  9.1 0.0 copy-start.2
  9.1 1.2 copy-done.2
  10.3 46.6 %shard_map.127 = (bf16[4,64,128]{2,1,0:T(8,128)(2,1)S(1)}, bf16[3,256,2048]{2,1,0:T(8,128)(2,1)S(1)}) custom-call(bf16[256,128]{1,0:T(8,128)(2,1)S(1)} %copy.50.q_ref, bf16[256,128]{1,0:T(8,128)(2,1)S(1)} %pad_maximum_fusion.1.kv_ref, bf16[256,2048]{1,0:T(8,128)(2,1)S(1)} %bitcast.21), custom_call_target="tpu_custom_call" | custom-call | flops 2147483648 | bytes 1048576 | tf_op jit(solution)/shard_map/pallas_call | solution.py:223
  56.9 0.0 copy-done.4
  56.9 0.0 copy-start.1
  56.9 1.6 %copy-done.1 = bf16[3,256,2048]{2,1,0:T(8,128)(2,1)} copy-done((bf16[3,256,2048]{2,1,0:T(8,128)(2,1)}, bf16[3,256,2048]{2,1,0:T(8,128)(2,1)S(1)}, u32[]{:S(2)}) %copy-start.1) | copy-done | bytes 3145752
  58.5 0.0 copy-start.3
  58.5 0.6 copy-done.3
  59.2 65.8 %shard_map.128 = bf16[64,2048]{1,0:T(8,128)(2,1)} custom-call(s32[192]{0:T(256)} %select_reduce_fusion.src_ref, s32[128]{0:T(128)} %copy-done.4, f32[128]{0:T(128)} %reshape.337.route_ref, bf16[4,64,128]{2,1,0:T(8,128)(2,1)} %copy-done.3, bf16[64,2048]{1,0:T(8,128)(2,1)} %resid_ref.1, bf16[512,2048]{1,0:T(8,128)(2,1)} %outw_ref.1, f32[1,2048]{1,0:T(1,128)} %bitcast.25, ...), custom_call_target="tpu_custom_call" | custom-call | flops 2415919104 | bytes 8388608 | tf_op jit(solution)/shard_map/pallas_call | solution.py:426
  125.0 1.7 %copy.52 = bf16[64,2048]{1,0:T(8,128)(2,1)} copy(bf16[64,2048]{1,0:T(8,128)(2,1)} %shard_map.128) | data formatting | bytes 524288
  (8 shorter events, 0.1 us)
Async XLA Ops:
  0.0 0.7 copy-start
  1.2 55.6 %copy-start.4 = (s32[128]{0:T(128)}, s32[128]{0:T(128)S(1)}, u32[]{:S(2)}) copy-start(s32[128]{0:T(128)S(1)} %get-tuple-element.24.slot_ref) | copy-start | bytes 1540
  9.1 1.2 copy-start.2
  56.9 1.7 %copy-start.1 = (bf16[3,256,2048]{2,1,0:T(8,128)(2,1)}, bf16[3,256,2048]{2,1,0:T(8,128)(2,1)S(1)}, u32[]{:S(2)}) copy-start(bf16[3,256,2048]{2,1,0:T(8,128)(2,1)S(1)} %get-tuple-element.8.others_ref) | copy-start | bytes 9437188
  58.5 0.6 copy-start.3

commit v3 on v0

v3 whole, which is shorter than its diff:
```python
import functools
import math

import jax
import jax.numpy as jnp
from jax import lax
from jax.experimental import pallas as pl
from jax.experimental.pallas import tpu as pltpu
from jax.sharding import PartitionSpec as P

HEAD_DIM = 64
TOPK = 2
GRID_W = 64
TOK_DEV = 256

eps = 1e-06
rope_base = 10000.0

LANES = 128
MESH = pl.DeviceIdType.MESH
NEAR = (0, 1, 7, 2, 6, 3, 5, 4)
GROUPS = (0, 2, 4, 5, 3, 6, 1, 7)
CHUNK = 512


def near_first(i):
    return lax.rem(8 + (2 * lax.rem(i, 2) - 1) * ((i + 1) // 2), 8)


def rotary_tables(sp):
    shape = (GRID_W + 8, LANES)
    freq_count = HEAD_DIM // 4
    lane = lax.broadcasted_iota(jnp.int32, shape, 1)
    item = lax.broadcasted_iota(jnp.int32, shape, 0)
    position = jnp.where(item < GRID_W, item, item - GRID_W + sp * (TOK_DEV // GRID_W)).astype(jnp.float32)
    index = lax.rem(lane, freq_count).astype(jnp.float32)
    angles = position * jnp.exp(index * (-math.log(rope_base) / freq_count))
    row_lane = lax.rem(lane[:GRID_W], 2 * freq_count) < freq_count

    def table(values):
        col = values[:GRID_W]
        return jnp.concatenate(
            [jnp.where(row_lane, values[GRID_W + r:GRID_W + r + 1], col) for r in range(TOK_DEV // GRID_W)], axis=0)

    return table(jnp.cos(angles)), table(jnp.sin(angles))


def prepare(values_f, gains, cosine, sine_table):
    lane = lax.broadcasted_iota(jnp.int32, values_f.shape, 1)
    low = lane < HEAD_DIM
    squares = values_f * values_f
    first = jnp.sum(jnp.where(low, squares, 0.0), axis=-1, keepdims=True)
    second = jnp.sum(jnp.where(low, 0.0, squares), axis=-1, keepdims=True)
    scale = jnp.where(low, lax.rsqrt(first / HEAD_DIM + eps), lax.rsqrt(second / HEAD_DIM + eps))
    normed = values_f * scale * gains
    half_dim = HEAD_DIM // 2
    turned = jnp.where(
        lax.rem(lane, HEAD_DIM) < half_dim, -pltpu.roll(normed, LANES - half_dim, 1), pltpu.roll(normed, half_dim, 1))
    return normed * cosine + turned * sine_table


def layer_kernel(
    src_ref, slot_ref, route_ref, query_ref, key_ref, value_ref, qgain_ref, kgain_ref, resid_ref, gain_ref,
    outw_hbm, gate_hbm, up_hbm, down_hbm,
    out_ref,
    qall, kvall, kk, vt, best_s, acc_s, osend, mlsend, orecv, mlrecv, attv, att,
    outw, gatew, upw, dcat, res3, normed3, sendbuf, recv, xall, hall, hsend, retsend, ret, out3,
    wsem, qs, qr, ks, kr, ps, pr, ms, mr, xs, xr, ds, dr,
    ss, sr, axs, axr, bxs, bxr, hs, hr, ts, tr,
):
    sp = lax.axis_index("sp")
    me_x = lax.axis_index("tp")
    z, j = sp // 8, lax.rem(sp, 8)
    right, left = lax.rem(me_x + 1, 4), lax.rem(me_x + 3, 4)
    tok = query_ref.shape[0]
    rows = resid_ref.shape[0]
    bf, f32 = jnp.bfloat16, jnp.float32

    def at_offset(dz, dj):
        return lax.rem(z + dz, 8) * 8 + lax.rem(j + dj, 8)

    def remote(src, dst, send, recv_sem, sp_to, x_to):
        return pltpu.make_async_remote_copy(
            src_ref=src, dst_ref=dst, send_sem=send, recv_sem=recv_sem,
            device_id=(sp_to, x_to), device_id_type=MESH)

    barrier = pltpu.get_barrier_semaphore()

    with jax.named_scope("greet"):
        for d in range(1, 4):
            pl.semaphore_signal(barrier, inc=1, device_id=(sp, lax.rem(me_x + d, 4)), device_id_type=MESH)
        for d in range(1, 8):
            for dz, dj in ((0, d), (d, 0)):
                pl.semaphore_signal(barrier, inc=1, device_id=(at_offset(dz, dj), me_x), device_id_type=MESH)

    weights = [
        pltpu.make_async_copy(a, b, wsem.at[n])
        for n, (a, b) in enumerate(((outw_hbm, outw), (gate_hbm, gatew), (up_hbm, upw), (down_hbm, dcat.at[0])))
    ]
    for copy in weights:
        copy.start()

    with jax.named_scope("prep"):
        lane = lax.broadcasted_iota(jnp.int32, (tok, LANES), 1)
        low = lane < HEAD_DIM
        cosine, sine_table = rotary_tables(sp)
        qgain = jnp.concatenate([qgain_ref[0:1, :], qgain_ref[1:2, :]], axis=1)
        qall[0] = prepare(query_ref[...].astype(f32), qgain, cosine, sine_table).astype(bf)
        key_value = jnp.concatenate([key_ref[...].astype(f32), value_ref[...].astype(f32)], axis=0).T
        kgain = jnp.concatenate([kgain_ref[...], kgain_ref[...]], axis=1)
        kvall[0] = jnp.where(low, prepare(key_value, kgain, cosine, sine_table), key_value).astype(bf)
        vt[HEAD_DIM:, :] = jnp.ones((16, vt.shape[1]), bf)
        best_s[...] = jnp.full(best_s.shape, -1e30, f32)
        acc_s[...] = jnp.zeros(acc_s.shape, f32)
    with jax.named_scope("barrier"):
        pl.semaphore_wait(barrier, 17)

    def q_copy(d):
        return remote(qall.at[0], qall.at[d], qs.at[d], qr.at[d], at_offset(0, d), me_x)

    def kv_copy(d):
        return remote(kvall.at[0], kvall.at[d], ks.at[d], kr.at[d], at_offset(d, 0), me_x)

    half = down_hbm.shape[0] // 2
    quarter = half // 2

    def down_copy(way):
        return remote(down_hbm, dcat.at[1 + 2 * way], ds.at[way], dr.at[way], sp, left if way == 0 else right)

    def down_pass(way, n):
        part = pl.ds(half * way + quarter * n, quarter)
        return remote(
            dcat.at[1 + 2 * way, part], dcat.at[2, part], ds.at[2 + 2 * n + way], dr.at[2 + 2 * n + way],
            sp, left if way == 0 else right)

    with jax.named_scope("issue"):
        for d in NEAR[1:]:
            kv_copy(d).start()
            q_copy(d).start()
        for way in range(2):
            down_copy(way).start()

    def spread(n):
        f = kvall[NEAR[n]].astype(f32)
        kk[n * tok:(n + 1) * tok, :] = jnp.where(low, f, pltpu.roll(f, HEAD_DIM, 1)).astype(bf)
        vt[0:HEAD_DIM, n * tok:(n + 1) * tok] = f.T[HEAD_DIM:, :].astype(bf)

    with jax.named_scope("spread1"):
        spread(0)
        for n in range(1, 4):
            with jax.named_scope(f"wait_kv{n}"):
                kv_copy(NEAR[n]).wait()
            spread(n)

    factor = math.log2(math.e) * HEAD_DIM ** (-0.5)

    def o_copy(d):
        return remote(osend.at[d], orecv.at[d], ps.at[d], pr.at[d], at_offset(0, 8 - d), me_x)

    def ml_copy(d):
        return remote(mlsend.at[d], mlrecv.at[d], ms.at[d], mr.at[d], at_offset(0, 8 - d), me_x)

    def second_half():
        for n in range(4, 8):
            with jax.named_scope(f"wait_kv{n}"):
                kv_copy(NEAR[n]).wait()
            spread(n)

    def down_turn():
        for way in range(2):
            down_copy(way).wait()
            down_pass(way, 0).start()

    def attend(i, carry):
        part = i // 8
        turn = lax.rem(i, 8)
        d = near_first(turn + part * (7 - 2 * turn))
        with jax.named_scope("wait_q"):
            pl.when((part == 0) & (d > 0))(lambda: q_copy(d).wait())
        pl.when(i == 8)(second_half)
        with jax.named_scope("down_turn"):
            pl.when(i == 14)(down_turn)
        with jax.named_scope("attend"):
            q = qall[d]
            zero = jnp.zeros_like(q)
            both = jnp.concatenate([jnp.where(low, q, zero), jnp.where(low, zero, q)], axis=0)
            best = best_s[d]
            acc = acc_s[d]
            for c in range(4 * tok // CHUNK):
                begin = pl.multiple_of(part * (4 * tok) + c * CHUNK, CHUNK)
                s = lax.dot_general(
                    kk[pl.ds(begin, CHUNK), :], both, (((1,), (1,)), ((), ())), preferred_element_type=f32)
                new = jnp.maximum(best, jnp.max(s, axis=0, keepdims=True))
                p = jnp.exp2((s - new) * factor).astype(bf)
                acc = acc * jnp.exp2((best - new) * factor) + jnp.dot(
                    vt[:, pl.ds(begin, CHUNK)], p, preferred_element_type=f32)
                best = new
            best_s[d] = best
            acc_s[d] = acc

        @pl.when(part == 1)
        def _():
            osend[d, 0:HEAD_DIM, :] = acc[0:HEAD_DIM, 0:tok].astype(bf)
            osend[d, HEAD_DIM:, :] = acc[0:HEAD_DIM, tok:].astype(bf)
            mlsend[d, 0:1, :] = best
            mlsend[d, 1:2, :] = acc[HEAD_DIM:HEAD_DIM + 1, :]

        @pl.when((part == 1) & (d > 0))
        def _():
            o_copy(d).start()
            ml_copy(d).start()

        return carry

    lax.fori_loop(0, 16, attend, 0)

    def finish(d, carry):
        ml_copy(d).wait()
        o_copy(d).wait()
        return carry

    with jax.named_scope("wait_part"):
        lax.fori_loop(1, 8, finish, 0)
    with jax.named_scope("combine"):
        tops = [mlsend[0, 0:1, :]] + [mlrecv[d, 0:1, :] for d in range(1, 8)]
        top = functools.reduce(jnp.maximum, tops)
        sums = jnp.zeros_like(top)
        heads = [jnp.zeros((HEAD_DIM, tok), f32) for _ in range(2)]
        for d in range(8):
            w = jnp.exp2((tops[d] - top) * factor)
            sums = sums + w * (mlsend[0, 1:2, :] if d == 0 else mlrecv[d, 1:2, :])
            o = (osend[0] if d == 0 else orecv[d]).astype(f32)
            for h in range(2):
                heads[h] = heads[h] + o[h * HEAD_DIM:(h + 1) * HEAD_DIM, :] * w[:, h * tok:(h + 1) * tok]
        full = jnp.concatenate([heads[h] / sums[:, h * tok:(h + 1) * tok] for h in range(2)], axis=0)
        joined = full.T.astype(bf)
        for x in range(4):
            attv[x] = joined[x * rows:(x + 1) * rows, :]

    def x_copy(d):
        to = lax.rem(me_x + d, 4)
        return remote(attv.at[to], att.at[me_x], xs.at[d], xr.at[d], sp, to)

    with jax.named_scope("x_exchange"):
        for d in (2, 1, 3):
            x_copy(d).start()
        att[me_x] = attv[me_x]
        weights[0].wait()
        for d in (1, 3, 2):
            x_copy(d).wait()
    for way in range(2):
        down_pass(way, 1).start()

    with jax.named_scope("proj"):
        mixed = jnp.zeros(resid_ref.shape, f32)
        for x in range(4):
            mixed = mixed + jnp.dot(att[x], outw[x * LANES:(x + 1) * LANES, :], preferred_element_type=f32)
        residual = (resid_ref[...].astype(f32) + mixed).astype(bf)
        resid_f = residual.astype(f32)
        scale = lax.rsqrt(jnp.mean(resid_f * resid_f, axis=-1, keepdims=True) + eps)
        normed = (resid_f * scale * gain_ref[...]).astype(bf)
        res3[...] = residual.reshape(rows, 16, LANES)
        normed3[...] = normed.reshape(rows, 16, LANES)

    def fill(i, carry):
        for k in range(3):
            sendbuf[i, k] = normed3[src_ref[3 * i + k]]
        return carry

    with jax.named_scope("fill"):
        lax.fori_loop(0, 64, fill, 0)

    with jax.named_scope("dispatch"):
        for dz in GROUPS:
            def dispatch(dj, carry, dz=dz):
                remote(sendbuf.at[dz * 8 + dj], recv.at[dz, dj], ss, sr.at[dz], at_offset(dz, dj), me_x).start()
                return carry

            lax.fori_loop(1 if dz == 0 else 0, 8, dispatch, 0)
        recv[0, 0] = sendbuf[0]

    def a_copy(dz, way):
        return remote(
            recv.at[dz], xall.at[2 * way, dz], axs.at[way, dz], axr.at[way, dz], sp, left if way == 0 else right)

    def b_copy(dz, way):
        part = pl.ds(4 * way, 4)
        return remote(
            xall.at[2 * way, dz, part], xall.at[1, dz, part], bxs.at[way, dz], bxr.at[way, dz],
            sp, left if way == 0 else right)

    def h_copy(dz, d):
        return remote(hsend.at[d, dz], hall.at[d, dz], hs.at[d, dz], hr.at[d, dz], sp, lax.rem(me_x + d, 4))

    def stage_a(dz):
        with jax.named_scope(f"A{dz}"):
            arrived = recv.at[0, pl.ds(1, 7)] if dz == 0 else recv.at[dz]
            pltpu.make_async_copy(arrived, arrived, sr.at[dz]).wait()
            for way in range(2):
                a_copy(dz, way).start()

    def stage_b(dz):
        with jax.named_scope(f"B{dz}"):
            for way in range(2):
                a_copy(dz, way).wait()
                b_copy(dz, way).start()

    def stage_c(pair):
        with jax.named_scope(f"Cw{pair[0]}"):
            for dz in pair:
                for way in range(2):
                    b_copy(dz, way).wait()
        with jax.named_scope(f"C{pair[0]}"):
            block = jnp.concatenate(
                [recv[dz].reshape(24, 16, LANES) for dz in pair]
                + [xall[d, dz].reshape(24, 16, LANES) for d in range(3) for dz in pair], axis=0)
            block = block.reshape(block.shape[0], 16 * LANES)
            gate = jnp.dot(block, gatew[...], preferred_element_type=f32)
            upper = jnp.dot(block, upw[...], preferred_element_type=f32)
            hidden = (gate / (1.0 + jnp.exp(-gate)) * upper).astype(bf)
            for n, dz in enumerate(pair):
                hall[0, dz] = hidden[24 * n:24 * (n + 1)]
                for d in range(1, 4):
                    begin = 24 * (len(pair) * d + n)
                    hsend[d, dz] = hidden[begin:begin + 24]
            for dz in pair:
                for d in range(1, 4):
                    h_copy(dz, d).start()

    def stage_d(pair):
        with jax.named_scope(f"Dw{pair[0]}"):
            for dz in pair:
                for d in range(1, 4):
                    h_copy(dz, d).wait()
        with jax.named_scope(f"D{pair[0]}"):
            full = None
            for d in range(4):
                hidden = jnp.concatenate([hall[d, dz] for dz in pair], axis=0)
                term = jnp.dot(hidden, dcat[(4 - d) % 4], preferred_element_type=f32)
                full = term if full is None else full + term
            tiles = full.astype(bf).reshape(len(pair), 8, 3, 16, LANES)
            for n, dz in enumerate(pair):
                retsend[dz] = tiles[n]
            for dz in pair:
                def give(dj, carry, dz=dz):
                    remote(
                        retsend.at[dz, dj], ret.at[pl.ds(24 * dz + 3 * dj, 3)], ts, tr,
                        at_offset(8 - dz, 8 - dj), me_x).start()
                    return carry

                if dz == 0:
                    ret[0:3] = retsend[0, 0]
                lax.fori_loop(1 if dz == 0 else 0, 8, give, 0)

    pairs = [GROUPS[n:n + 2] for n in range(0, 8, 2)]

    def both_of(stage, n):
        for dz in pairs[n]:
            stage(dz)

    def wait_down():
        with jax.named_scope("wait_down"):
            weights[3].wait()
            for way in range(2):
                for n in range(2):
                    down_pass(way, n).wait()

    both_of(stage_a, 0)
    both_of(stage_b, 0)
    both_of(stage_a, 1)
    weights[1].wait()
    weights[2].wait()
    stage_c(pairs[0])
    both_of(stage_b, 1)
    both_of(stage_a, 2)
    wait_down()
    stage_d(pairs[0])
    stage_c(pairs[1])
    both_of(stage_b, 2)
    both_of(stage_a, 3)
    stage_d(pairs[1])
    stage_c(pairs[2])
    both_of(stage_b, 3)
    stage_d(pairs[2])
    stage_c(pairs[3])
    stage_d(pairs[3])

    with jax.named_scope("wait_ret"):
        pltpu.make_async_copy(ret.at[pl.ds(3, 189)], ret.at[pl.ds(3, 189)], tr).wait()

    def join(t, carry):
        both = jnp.zeros((16, LANES), f32)
        for k in range(TOPK):
            both = both + ret[slot_ref[TOPK * t + k]].astype(f32) * route_ref[k, t]
        out3[t] = (res3[t].astype(f32) + both).astype(bf)
        return carry

    with jax.named_scope("join"):
        lax.fori_loop(0, rows, join, 0)
        out_ref[...] = out3[...].reshape(rows, 16 * LANES)
    pltpu.make_async_copy(sendbuf.at[pl.ds(1, 63)], sendbuf.at[pl.ds(1, 63)], ss).wait()
    pltpu.make_async_copy(sendbuf.at[pl.ds(1, 63)], sendbuf.at[pl.ds(1, 63)], ts).wait()


def routing(own_ids):
    sp = lax.axis_index("sp")
    flat = own_ids.reshape(-1)
    count = flat.shape[0]
    item = jnp.arange(count, dtype=jnp.int32)
    earlier = (flat[:, None] == flat[None, :]) & (item[None, :] < item[:, None])
    rank = jnp.sum(earlier.astype(jnp.int32), axis=1)
    place = ((flat // 8 - sp // 8) % 8) * 8 + (flat - sp) % 8
    slot = place * 3 + rank
    named = jnp.arange(192, dtype=jnp.int32)[:, None] == slot[None, :]
    src = jnp.sum(jnp.where(named, item[None, :] // TOPK, 0), axis=1)
    return slot, src


def body(
    resid_in,
    query_proj,
    key_proj,
    value_proj,
    query_gain,
    key_gain,
    out_weight,
    norm_gain,
    gate_weight,
    up_weight,
    down_weight,
    expert_ids,
    route_weight,
):
    tok = query_proj.shape[0]
    rows = resid_in.shape[0]
    own_ids = lax.dynamic_slice_in_dim(expert_ids, lax.axis_index("tp") * rows, rows, 0)
    slot, src = routing(own_ids)
    ff = down_weight.shape[1]
    bf, f32 = jnp.bfloat16, jnp.float32
    dma = pltpu.SemaphoreType.DMA
    smem = pl.BlockSpec(memory_space=pltpu.SMEM)
    vmem = pl.BlockSpec(memory_space=pltpu.VMEM)
    hbm = pl.BlockSpec(memory_space=pl.ANY)
    return pl.pallas_call(
        layer_kernel,
        out_shape=jax.ShapeDtypeStruct(resid_in.shape, bf),
        in_specs=[smem] * 3 + [vmem] * 7 + [hbm] * 4,
        out_specs=vmem,
        scratch_shapes=[
            pltpu.VMEM((8, tok, LANES), bf),
            pltpu.VMEM((8, tok, LANES), bf),
            pltpu.VMEM((8 * tok, LANES), bf),
            pltpu.VMEM((HEAD_DIM + 16, 8 * tok), bf),
            pltpu.VMEM((8, 1, 2 * tok), f32),
            pltpu.VMEM((8, HEAD_DIM + 16, 2 * tok), f32),
            pltpu.VMEM((8, LANES, tok), bf),
            pltpu.VMEM((8, 2, 2 * tok), f32),
            pltpu.VMEM((8, LANES, tok), bf),
            pltpu.VMEM((8, 2, 2 * tok), f32),
            pltpu.VMEM((4, rows, LANES), bf),
            pltpu.VMEM((4, rows, LANES), bf),
            pltpu.VMEM(out_weight.shape, bf),
            pltpu.VMEM(gate_weight.shape[1:], bf),
            pltpu.VMEM(up_weight.shape[1:], bf),
            pltpu.VMEM((4,) + down_weight.shape[1:], bf),
            pltpu.VMEM((rows, 16, LANES), bf),
            pltpu.VMEM((rows, 16, LANES), bf),
            pltpu.VMEM((64, 3, 16, LANES), bf),
            pltpu.VMEM((8, 8, 3, 16, LANES), bf),
            pltpu.VMEM((3, 8, 8, 3, 16, LANES), bf),
            pltpu.VMEM((4, 8, 24, ff), bf),
            pltpu.VMEM((4, 8, 24, ff), bf),
            pltpu.VMEM((8, 8, 3, 16, LANES), bf),
            pltpu.VMEM((192, 16, LANES), bf),
            pltpu.VMEM((rows, 16, LANES), bf),
        ] + [dma((4,))] + [dma((8,))] * 8 + [dma((4,))] * 2 + [dma((6,))] * 2
        + [dma(()), dma((8,))] + [dma((2, 8))] * 4 + [dma((4, 8))] * 2 + [dma(())] * 2,
        compiler_params=pltpu.CompilerParams(
            collective_id=0, has_side_effects=True, vmem_limit_bytes=60 << 20),
    )(
        src, slot, route_weight.T, query_proj, key_proj.T, value_proj.T, query_gain, key_gain, resid_in,
        norm_gain[None], out_weight, gate_weight[0], up_weight[0], down_weight[0],
    )


def solution(mesh):
    placed = (
        P(("sp", "tp"), None),
        P("sp", "tp"),
        P("sp", "tp"),
        P("sp", "tp"),
        P("tp", None),
        P("tp", None),
        P(),
        P(),
        P("sp", None, "tp"),
        P("sp", None, "tp"),
        P("sp", "tp", None),
        P("sp", None),
        P(("sp", "tp"), None),
    )
    return jax.shard_map(
        body, mesh=mesh, in_specs=placed, out_specs=P(("sp", "tp"), None), check_vma=False
    )
```

time: 369 us -> 107 us (0.29)
  waiting for transfers between devices: 146 us -> 0 us
  Pallas kernels: 0 us -> 103 us
  blocking collectives: 77.2 us -> 0 us
  matrix products: 62.2 us -> 0 us
  local copies, waits for them, and re-layouts: 37.6 us -> 2.66 us
  starting transfers between devices: 16.2 us -> 0 us
  other arithmetic: 15.2 us -> 0.88 us
  between operations: 13.7 us -> 0.03 us
    all_gather x2 -> x0, waiting for transfers between devices: 114 us -> none  [the longest x1 77.1 us: side_by_side(): lax.all_gather(both, axis, axis=dim, tiled=True)]
    pallas_call x0 -> x1, Pallas kernels: none -> 103 us  [body(): pl.pallas_call(layer_kernel, out_shape=jax.ShapeDtypeStruct(resid_in.shap...]
    all_to_all x2 -> x0, blocking collectives: 77.2 us -> none  [the longest x1 39.2 us: summed_on_arrival(): lax.all_to_all(in_blocks(value, dim, devices), axis, 0, 0, tiled=True)]
    dot_general x21 -> x0, matrix products: 62.2 us -> none  [the longest x8 29 us: attend_piece(): jnp.einsum('qkgd,skd->qkgs', grouped, seg_keys, preferred_element_type=jn...]
    all_to_all x2 -> x0, waiting for transfers between devices: 31.8 us -> none  [the longest x1 27.4 us: body(): lax.all_to_all(expert_out, 'sp', split_axis=0, concat_axis=0, tiled=True)]
    reshape x8 -> x1, local copies, waits for them, and re-layouts: 17.7 us -> 0.14 us  [routing(): flat = own_ids.reshape(-1)]
    all_to_all x2 -> x0, starting transfers between devices: 16.2 us -> none  [the longest x1 12.2 us: body(): lax.all_to_all(expert_out, 'sp', split_axis=0, concat_axis=0, tiled=True)]
    reduce_sum x13 -> x2, other arithmetic: 9.61 us -> 0.86 us  [the longest x1 0.68 us: routing(): src = jnp.sum(jnp.where(named, item[None, :] // TOPK, 0), axis=1)]
  transfers between devices with their start and end apart: 4 -> 0, of which waited for: 4 -> 0; matrix products, arithmetic and copies ran while one was open for 1% -> 0% of each run, Pallas kernels for 0% -> 0%
where the time goes in v3:
time: 107 us
  Pallas kernels  103 us (96%)
  local copies, waits for them, and re-layouts  2.66 us (2%)
    pallas_call x1, Pallas kernels, body(): pl.pallas_call(layer_kernel, out_shape=jax.ShapeDtypeStruct(resid_in.shap...  103 us
    unnamed x5, local copies, waits for them, and re-layouts  2.36 us

profile of v3, /device:TPU:1, one launch (start us, length us, event | category | flops | bytes accessed | tf_op | source)
XLA Modules:
  0.0 106.8 jit_solution(15338789769068944662)
XLA Ops:
  0.0 0.0 copy-start
  0.0 0.7 copy-done
  0.7 0.1 constant_dynamic-slice_fusion
  0.8 0.1 copy.16
  0.9 0.1 reshape.103
  1.0 0.2 convert_reduce_fusion
  1.2 0.0 copy-start.1
  1.2 0.7 select_reduce_fusion.src_ref
  1.9 0.0 copy-done.1
  1.9 103.2 %shard_map.127 = bf16[64,2048]{1,0:T(8,128)(2,1)} custom-call(s32[192]{0:T(256)} %select_reduce_fusion.src_ref, s32[128]{0:T(128)} %copy-done.1, f32[2,64]{1,0:T(2,128)} %bitcast.13, bf16[256,128]{1,0:T(8,128)(2,1)} %query_ref.1, bf16[64,256]{1,0:T(8,128)(2,1)} %bitcast.10, bf16[64,256]{1,0:T(8,128)(2,1)} %bitcast.11, f32[2,64]{1,0:T(2,128)} %qgain_ref.1, ...), custom_call_target="tpu_custom_call" | custom-call | tf_op jit(solution)/shard_map/pallas_call | solution.py:444
  105.1 1.7 %copy.18 = bf16[64,2048]{1,0:T(8,128)(2,1)} copy(bf16[64,2048]{1,0:T(8,128)(2,1)} %shard_map.127) | data formatting | bytes 524288
  (1 shorter events, 0.0 us)
Async XLA Ops:
  0.0 0.7 copy-start
  1.2 0.7 copy-start.1

commit v4 on v3

--- a/solution.py
+++ b/solution.py
@@ -19,8 +19,9 @@
 LANES = 128
 MESH = pl.DeviceIdType.MESH
 NEAR = (0, 1, 7, 2, 6, 3, 5, 4)
-GROUPS = (0, 2, 4, 5, 3, 6, 1, 7)
-CHUNK = 512
+LEAD = 3
+GROUPS = (0, 1, 4, 5, 3, 6, 2, 7)
+PARTS = (((0, 512), (512, 256)), ((768, 512),), ((1280, 512), (1792, 256)))
 
 
 def near_first(i):
@@ -60,11 +61,11 @@
 
 
 def layer_kernel(
-    src_ref, slot_ref, route_ref, query_ref, key_ref, value_ref, qgain_ref, kgain_ref, resid_ref, gain_ref,
+    ids_ref, route_ref, query_ref, key_ref, value_ref, qgain_ref, kgain_ref, resid_ref, gain_ref,
     outw_hbm, gate_hbm, up_hbm, down_hbm,
     out_ref,
     qall, kvall, kk, vt, best_s, acc_s, osend, mlsend, orecv, mlrecv, attv, att,
-    outw, gatew, upw, dcat, res3, normed3, sendbuf, recv, xall, hall, hsend, retsend, ret, out3,
+    outw, gatew, upw, dcat, pick, joiner, resid_s, sendbuf, recv, xall, hall, hsend, retsend, ret,
     wsem, qs, qr, ks, kr, ps, pr, ms, mr, xs, xr, ds, dr,
     ss, sr, axs, axr, bxs, bxr, hs, hr, ts, tr,
 ):
@@ -110,8 +111,6 @@
         kgain = jnp.concatenate([kgain_ref[...], kgain_ref[...]], axis=1)
         kvall[0] = jnp.where(low, prepare(key_value, kgain, cosine, sine_table), key_value).astype(bf)
         vt[HEAD_DIM:, :] = jnp.ones((16, vt.shape[1]), bf)
-        best_s[...] = jnp.full(best_s.shape, -1e30, f32)
-        acc_s[...] = jnp.zeros(acc_s.shape, f32)
     with jax.named_scope("barrier"):
         pl.semaphore_wait(barrier, 17)
 
@@ -122,7 +121,7 @@
         return remote(kvall.at[0], kvall.at[d], ks.at[d], kr.at[d], at_offset(d, 0), me_x)
 
     half = down_hbm.shape[0] // 2
-    quarter = half // 2
+    quarter = half // 4
 
     def down_copy(way):
         return remote(down_hbm, dcat.at[1 + 2 * way], ds.at[way], dr.at[way], sp, left if way == 0 else right)
@@ -134,9 +133,12 @@
             sp, left if way == 0 else right)
 
     with jax.named_scope("issue"):
+        for d in NEAR[1:3]:
+            kv_copy(d).start()
         for d in NEAR[1:]:
+            q_copy(d).start()
+        for d in NEAR[3:]:
             kv_copy(d).start()
-            q_copy(d).start()
         for way in range(2):
             down_copy(way).start()
 
@@ -145,9 +147,31 @@
         kk[n * tok:(n + 1) * tok, :] = jnp.where(low, f, pltpu.roll(f, HEAD_DIM, 1)).astype(bf)
         vt[0:HEAD_DIM, n * tok:(n + 1) * tok] = f.T[HEAD_DIM:, :].astype(bf)
 
+    with jax.named_scope("routing"):
+        ids = ids_ref[0:2, 0:rows]
+        for x in range(1, 4):
+            ids = jnp.where(me_x == x, ids_ref[0:2, x * rows:(x + 1) * rows], ids)
+        ids = ids.astype(f32)
+        items = TOPK * rows
+        flat = jnp.broadcast_to(jnp.concatenate([ids[0:1], ids[1:2]], axis=1), (items, items))
+        turned = flat.T
+        same = flat == turned
+        first = lax.broadcasted_iota(jnp.int32, (items, items), 0)
+        second = lax.broadcasted_iota(jnp.int32, (items, items), 1)
+
+        def slot_of(e, rank):
+            e = e.astype(jnp.int32)
+            place = lax.rem(lax.div(e, 8) + 8 - z, 8) * 8 + lax.rem(lax.rem(e, 8) + 8 - j, 8)
+            return place * 3 + rank.astype(jnp.int32)
+
+        across = slot_of(flat[0:1], jnp.sum(jnp.where(same & (first < second), 1.0, 0.0), axis=0, keepdims=True))
+        down = slot_of(turned[:, 0:1], jnp.sum(jnp.where(same & (second < first), 1.0, 0.0), axis=1, keepdims=True))
+        pick[...] = jnp.where(lax.broadcasted_iota(jnp.int32, pick.shape, 0) == across, 1.0, 0.0).astype(bf)
+        joiner[...] = jnp.where(lax.broadcasted_iota(jnp.int32, joiner.shape, 1) == down, 1.0, 0.0).astype(bf)
+
     with jax.named_scope("spread1"):
         spread(0)
-        for n in range(1, 4):
+        for n in range(1, 3):
             with jax.named_scope(f"wait_kv{n}"):
                 kv_copy(NEAR[n]).wait()
             spread(n)
@@ -160,59 +184,74 @@
     def ml_copy(d):
         return remote(mlsend.at[d], mlrecv.at[d], ms.at[d], mr.at[d], at_offset(0, 8 - d), me_x)
 
-    def second_half():
-        for n in range(4, 8):
-            with jax.named_scope(f"wait_kv{n}"):
-                kv_copy(NEAR[n]).wait()
-            spread(n)
-
-    def down_turn():
+    def pass_on(n):
         for way in range(2):
-            down_copy(way).wait()
-            down_pass(way, 0).start()
-
-    def attend(i, carry):
-        part = i // 8
-        turn = lax.rem(i, 8)
-        d = near_first(turn + part * (7 - 2 * turn))
-        with jax.named_scope("wait_q"):
-            pl.when((part == 0) & (d > 0))(lambda: q_copy(d).wait())
-        pl.when(i == 8)(second_half)
-        with jax.named_scope("down_turn"):
-            pl.when(i == 14)(down_turn)
+            down_pass(way, n).start()
+
+    def attend(d, spans, best, acc):
         with jax.named_scope("attend"):
             q = qall[d]
             zero = jnp.zeros_like(q)
             both = jnp.concatenate([jnp.where(low, q, zero), jnp.where(low, zero, q)], axis=0)
-            best = best_s[d]
-            acc = acc_s[d]
-            for c in range(4 * tok // CHUNK):
-                begin = pl.multiple_of(part * (4 * tok) + c * CHUNK, CHUNK)
-                s = lax.dot_general(
-                    kk[pl.ds(begin, CHUNK), :], both, (((1,), (1,)), ((), ())), preferred_element_type=f32)
-                new = jnp.maximum(best, jnp.max(s, axis=0, keepdims=True))
+
+            def scores(span):
+                return lax.dot_general(
+                    kk[span[0]:span[0] + span[1], :], both, (((1,), (1,)), ((), ())), preferred_element_type=f32)
+
+            s = scores(spans[0])
+            for n, (begin, size) in enumerate(spans):
+                ahead = scores(spans[n + 1]) if n + 1 < len(spans) else None
+                new = jnp.max(s, axis=0, keepdims=True)
+                if best is not None:
+                    new = jnp.maximum(best, new)
                 p = jnp.exp2((s - new) * factor).astype(bf)
-                acc = acc * jnp.exp2((best - new) * factor) + jnp.dot(
-                    vt[:, pl.ds(begin, CHUNK)], p, preferred_element_type=f32)
-                best = new
-            best_s[d] = best
-            acc_s[d] = acc
-
-        @pl.when(part == 1)
-        def _():
-            osend[d, 0:HEAD_DIM, :] = acc[0:HEAD_DIM, 0:tok].astype(bf)
-            osend[d, HEAD_DIM:, :] = acc[0:HEAD_DIM, tok:].astype(bf)
-            mlsend[d, 0:1, :] = best
-            mlsend[d, 1:2, :] = acc[HEAD_DIM:HEAD_DIM + 1, :]
-
-        @pl.when((part == 1) & (d > 0))
+                part = jnp.dot(vt[:, begin:begin + size], p, preferred_element_type=f32)
+                acc = part if best is None else acc * jnp.exp2((best - new) * factor) + part
+                best, s = new, ahead
+            return best, acc
+
+    def early(i, carry):
+        d = near_first(i)
+        with jax.named_scope("wait_q"):
+            pl.when(d > 0)(lambda: q_copy(d).wait())
+        best, acc = attend(d, PARTS[0], None, None)
+        best_s[d] = best
+        acc_s[d] = acc
+        return carry
+
+    def middle(d, carry):
+        best, acc = attend(d, PARTS[1], best_s[d], acc_s[d])
+        best_s[d] = best
+        acc_s[d] = acc
+        return carry
+
+    lax.fori_loop(0, 8, early, 0)
+    with jax.named_scope("spread2"):
+        for n in range(3, 5):
+            kv_copy(NEAR[n]).wait()
+            spread(n)
+    lax.fori_loop(0, 8, middle, 0)
+    with jax.named_scope("spread3"):
+        for n in range(5, 8):
+            kv_copy(NEAR[n]).wait()
+            spread(n)
+
+    def late(i, carry):
+        d = near_first(7 - i)
+        best, acc = attend(d, PARTS[2], best_s[d], acc_s[d])
+        osend[d, 0:HEAD_DIM, :] = acc[0:HEAD_DIM, 0:tok].astype(bf)
+        osend[d, HEAD_DIM:, :] = acc[0:HEAD_DIM, tok:].astype(bf)
+        mlsend[d, 0:1, :] = best
+        mlsend[d, 1:2, :] = acc[HEAD_DIM:HEAD_DIM + 1, :]
+
+        @pl.when(d > 0)
         def _():
             o_copy(d).start()
             ml_copy(d).start()
 
         return carry
 
-    lax.fori_loop(0, 16, attend, 0)
+    lax.fori_loop(0, 8, late, 0)
 
     def finish(d, carry):
         ml_copy(d).wait()
@@ -244,13 +283,14 @@
     with jax.named_scope("x_exchange"):
         for d in (2, 1, 3):
             x_copy(d).start()
+        for way in range(2):
+            down_copy(way).wait()
+        for n in range(4):
+            pass_on(n)
         att[me_x] = attv[me_x]
         weights[0].wait()
         for d in (1, 3, 2):
             x_copy(d).wait()
-    for way in range(2):
-        down_pass(way, 1).start()
-
     with jax.named_scope("proj"):
         mixed = jnp.zeros(resid_ref.shape, f32)
         for x in range(4):
@@ -259,24 +299,22 @@
         resid_f = residual.astype(f32)
         scale = lax.rsqrt(jnp.mean(resid_f * resid_f, axis=-1, keepdims=True) + eps)
         normed = (resid_f * scale * gain_ref[...]).astype(bf)
-        res3[...] = residual.reshape(rows, 16, LANES)
-        normed3[...] = normed.reshape(rows, 16, LANES)
-
-    def fill(i, carry):
-        for k in range(3):
-            sendbuf[i, k] = normed3[src_ref[3 * i + k]]
-        return carry
+        resid_s[...] = residual
 
     with jax.named_scope("fill"):
-        lax.fori_loop(0, 64, fill, 0)
+        chosen = jnp.dot(pick[...], jnp.concatenate([normed, normed], axis=0), preferred_element_type=f32)
+        sendbuf[...] = chosen.astype(bf).reshape(64, 3, 16, LANES)
+
+    def dispatch(dz):
+        def send(dj, carry):
+            remote(sendbuf.at[dz * 8 + dj], recv.at[dz, dj], ss, sr.at[dz], at_offset(dz, dj), me_x).start()
+            return carry
+
+        lax.fori_loop(1 if dz == 0 else 0, 8, send, 0)
 
     with jax.named_scope("dispatch"):
-        for dz in GROUPS:
-            def dispatch(dj, carry, dz=dz):
-                remote(sendbuf.at[dz * 8 + dj], recv.at[dz, dj], ss, sr.at[dz], at_offset(dz, dj), me_x).start()
-                return carry
-
-            lax.fori_loop(1 if dz == 0 else 0, 8, dispatch, 0)
+        for dz in GROUPS[:LEAD]:
+            dispatch(dz)
         recv[0, 0] = sendbuf[0]
 
     def a_copy(dz, way):
@@ -298,6 +336,9 @@
             pltpu.make_async_copy(arrived, arrived, sr.at[dz]).wait()
             for way in range(2):
                 a_copy(dz, way).start()
+            after = GROUPS.index(dz) + LEAD
+            if after < 8:
+                dispatch(GROUPS[after])
 
     def stage_b(dz):
         with jax.named_scope(f"B{dz}"):
@@ -354,66 +395,54 @@
 
     pairs = [GROUPS[n:n + 2] for n in range(0, 8, 2)]
 
-    def both_of(stage, n):
-        for dz in pairs[n]:
-            stage(dz)
-
     def wait_down():
         with jax.named_scope("wait_down"):
             weights[3].wait()
             for way in range(2):
-                for n in range(2):
+                for n in range(4):
                     down_pass(way, n).wait()
 
-    both_of(stage_a, 0)
-    both_of(stage_b, 0)
-    both_of(stage_a, 1)
+    g = GROUPS
+    stage_a(g[0])
+    stage_a(g[1])
+    stage_b(g[0])
+    stage_a(g[2])
+    stage_b(g[1])
+    stage_a(g[3])
+    stage_b(g[2])
     weights[1].wait()
     weights[2].wait()
     stage_c(pairs[0])
-    both_of(stage_b, 1)
-    both_of(stage_a, 2)
+    stage_a(g[4])
+    stage_b(g[3])
+    stage_a(g[5])
+    stage_b(g[4])
     wait_down()
     stage_d(pairs[0])
     stage_c(pairs[1])
-    both_of(stage_b, 2)
-    both_of(stage_a, 3)
+    stage_a(g[6])
+    stage_b(g[5])
+    stage_a(g[7])
+    stage_b(g[6])
     stage_d(pairs[1])
     stage_c(pairs[2])
-    both_of(stage_b, 3)
+    stage_c(g[6:7])
+    stage_b(g[7])
     stage_d(pairs[2])
-    stage_c(pairs[3])
-    stage_d(pairs[3])
+    stage_c(g[7:8])
+    stage_d(g[6:7])
+    stage_d(g[7:8])
 
     with jax.named_scope("wait_ret"):
         pltpu.make_async_copy(ret.at[pl.ds(3, 189)], ret.at[pl.ds(3, 189)], tr).wait()
 
-    def join(t, carry):
-        both = jnp.zeros((16, LANES), f32)
-        for k in range(TOPK):
-            both = both + ret[slot_ref[TOPK * t + k]].astype(f32) * route_ref[k, t]
-        out3[t] = (res3[t].astype(f32) + both).astype(bf)
-        return carry
-
     with jax.named_scope("join"):
-        lax.fori_loop(0, rows, join, 0)
-        out_ref[...] = out3[...].reshape(rows, 16 * LANES)
+        picked = jnp.dot(joiner[...], ret[...].reshape(192, 16 * LANES), preferred_element_type=f32)
+        share = route_ref[...].T
+        both = picked[0:rows] * share[:, 0:1] + picked[rows:] * share[:, 1:2]
+        out_ref[...] = (resid_s[...].astype(f32) + both).astype(bf)
     pltpu.make_async_copy(sendbuf.at[pl.ds(1, 63)], sendbuf.at[pl.ds(1, 63)], ss).wait()
     pltpu.make_async_copy(sendbuf.at[pl.ds(1, 63)], sendbuf.at[pl.ds(1, 63)], ts).wait()
-
-
-def routing(own_ids):
-    sp = lax.axis_index("sp")
-    flat = own_ids.reshape(-1)
-    count = flat.shape[0]
-    item = jnp.arange(count, dtype=jnp.int32)
-    earlier = (flat[:, None] == flat[None, :]) & (item[None, :] < item[:, None])
-    rank = jnp.sum(earlier.astype(jnp.int32), axis=1)
-    place = ((flat // 8 - sp // 8) % 8) * 8 + (flat - sp) % 8
-    slot = place * 3 + rank
-    named = jnp.arange(192, dtype=jnp.int32)[:, None] == slot[None, :]
-    src = jnp.sum(jnp.where(named, item[None, :] // TOPK, 0), axis=1)
-    return slot, src
 
 
 def body(
@@ -433,18 +462,15 @@
 ):
     tok = query_proj.shape[0]
     rows = resid_in.shape[0]
-    own_ids = lax.dynamic_slice_in_dim(expert_ids, lax.axis_index("tp") * rows, rows, 0)
-    slot, src = routing(own_ids)
     ff = down_weight.shape[1]
     bf, f32 = jnp.bfloat16, jnp.float32
     dma = pltpu.SemaphoreType.DMA
-    smem = pl.BlockSpec(memory_space=pltpu.SMEM)
     vmem = pl.BlockSpec(memory_space=pltpu.VMEM)
     hbm = pl.BlockSpec(memory_space=pl.ANY)
     return pl.pallas_call(
         layer_kernel,
         out_shape=jax.ShapeDtypeStruct(resid_in.shape, bf),
-        in_specs=[smem] * 3 + [vmem] * 7 + [hbm] * 4,
+        in_specs=[vmem] * 9 + [hbm] * 4,
         out_specs=vmem,
         scratch_shapes=[
             pltpu.VMEM((8, tok, LANES), bf),
@@ -463,8 +489,9 @@
             pltpu.VMEM(gate_weight.shape[1:], bf),
             pltpu.VMEM(up_weight.shape[1:], bf),
             pltpu.VMEM((4,) + down_weight.shape[1:], bf),
-            pltpu.VMEM((rows, 16, LANES), bf),
-            pltpu.VMEM((rows, 16, LANES), bf),
+            pltpu.VMEM((192, TOPK * rows), bf),
+            pltpu.VMEM((TOPK * rows, 192), bf),
+            pltpu.VMEM(resid_in.shape, bf),
             pltpu.VMEM((64, 3, 16, LANES), bf),
             pltpu.VMEM((8, 8, 3, 16, LANES), bf),
             pltpu.VMEM((3, 8, 8, 3, 16, LANES), bf),
@@ -472,13 +499,12 @@
             pltpu.VMEM((4, 8, 24, ff), bf),
             pltpu.VMEM((8, 8, 3, 16, LANES), bf),
             pltpu.VMEM((192, 16, LANES), bf),
-            pltpu.VMEM((rows, 16, LANES), bf),
-        ] + [dma((4,))] + [dma((8,))] * 8 + [dma((4,))] * 2 + [dma((6,))] * 2
+        ] + [dma((4,))] + [dma((8,))] * 8 + [dma((4,))] * 2 + [dma((10,))] * 2
         + [dma(()), dma((8,))] + [dma((2, 8))] * 4 + [dma((4, 8))] * 2 + [dma(())] * 2,
         compiler_params=pltpu.CompilerParams(
             collective_id=0, has_side_effects=True, vmem_limit_bytes=60 << 20),
     )(
-        src, slot, route_weight.T, query_proj, key_proj.T, value_proj.T, query_gain, key_gain, resid_in,
+        expert_ids.T, route_weight.T, query_proj, key_proj.T, value_proj.T, query_gain, key_gain, resid_in,
         norm_gain[None], out_weight, gate_weight[0], up_weight[0], down_weight[0],
     )
 

time: 107 us -> 99.1 us (0.926)
  Pallas kernels: 103 us -> 97.3 us
    pallas_call x1, Pallas kernels: 103 us -> 97.3 us  [body(): pl.pallas_call(layer_kernel, out_shape=jax.ShapeDtypeStruct(resid_in.shap...]
    unnamed x5 -> x1, local copies, waits for them, and re-layouts: 2.36 us -> 1.67 us
where the time goes in v4:
time: 99.1 us; the launch traced here: 99 us
  Pallas kernels  97.3 us (98%)
  local copies, waits for them, and re-layouts  1.67 us (2%)
    pallas_call x1, Pallas kernels, body(): pl.pallas_call(layer_kernel, out_shape=jax.ShapeDtypeStruct(resid_in.shap...  97.3 us

profile of v4, /device:TPU:1, one launch (start us, length us, event | category | flops | bytes accessed | tf_op | source)
XLA Modules:
  0.0 99.0 jit_solution(10078717527142916588)
XLA Ops:
  0.0 97.3 %shard_map.127 = bf16[64,2048]{1,0:T(8,128)(2,1)} custom-call(s32[2,256]{1,0:T(2,128)} %bitcast.14, f32[2,64]{1,0:T(2,128)} %bitcast.15, bf16[256,128]{1,0:T(8,128)(2,1)} %query_ref.1, bf16[64,256]{1,0:T(8,128)(2,1)} %bitcast.11, bf16[64,256]{1,0:T(8,128)(2,1)} %bitcast.12, f32[2,64]{1,0:T(2,128)} %qgain_ref.1, f32[1,64]{1,0:T(1,128)} %kgain_ref.1, ...), custom_call_target="tpu_custom_call" | custom-call | tf_op jit(solution)/shard_map/pallas_call | solution.py:470
  97.3 1.7 %copy.15 = bf16[64,2048]{1,0:T(8,128)(2,1)} copy(bf16[64,2048]{1,0:T(8,128)(2,1)} %shard_map.127) | data formatting | bytes 524288

commit v5 on v4

--- a/solution.py
+++ b/solution.py
@@ -19,8 +19,8 @@
 LANES = 128
 MESH = pl.DeviceIdType.MESH
 NEAR = (0, 1, 7, 2, 6, 3, 5, 4)
-LEAD = 3
-GROUPS = (0, 1, 4, 5, 3, 6, 2, 7)
+PACE = ((0, 1, 2), (3,), (4,), (5,), (6,), (7,), (), (), ())
+GROUPS = (0, 1, 5, 3, 4, 6, 2, 7)
 PARTS = (((0, 512), (512, 256)), ((768, 512),), ((1280, 512), (1792, 256)))
 
 
@@ -137,7 +137,7 @@
             kv_copy(d).start()
         for d in NEAR[1:]:
             q_copy(d).start()
-        for d in NEAR[3:]:
+        for d in NEAR[3:5]:
             kv_copy(d).start()
         for way in range(2):
             down_copy(way).start()
@@ -174,6 +174,9 @@
         for n in range(1, 3):
             with jax.named_scope(f"wait_kv{n}"):
                 kv_copy(NEAR[n]).wait()
+            if n == 1:
+                for d in NEAR[5:]:
+                    kv_copy(d).start()
             spread(n)
 
     factor = math.log2(math.e) * HEAD_DIM ** (-0.5)
@@ -252,6 +255,10 @@
         return carry
 
     lax.fori_loop(0, 8, late, 0)
+    with jax.named_scope("down_turn"):
+        for way in range(2):
+            down_copy(way).wait()
+        pass_on(0)
 
     def finish(d, carry):
         ml_copy(d).wait()
@@ -283,9 +290,7 @@
     with jax.named_scope("x_exchange"):
         for d in (2, 1, 3):
             x_copy(d).start()
-        for way in range(2):
-            down_copy(way).wait()
-        for n in range(4):
+        for n in range(1, 4):
             pass_on(n)
         att[me_x] = attv[me_x]
         weights[0].wait()
@@ -313,8 +318,8 @@
         lax.fori_loop(1 if dz == 0 else 0, 8, send, 0)
 
     with jax.named_scope("dispatch"):
-        for dz in GROUPS[:LEAD]:
-            dispatch(dz)
+        for n in PACE[0]:
+            dispatch(GROUPS[n])
         recv[0, 0] = sendbuf[0]
 
     def a_copy(dz, way):
@@ -326,6 +331,10 @@
         return remote(
             xall.at[2 * way, dz, part], xall.at[1, dz, part], bxs.at[way, dz], bxr.at[way, dz],
             sp, left if way == 0 else right)
+
+    def far_copy(dz):
+        return remote(
+            recv.at[dz], xall.at[1, dz], bxs.at[0, dz], bxr.at[0, dz], sp, lax.rem(me_x + 2, 4))
 
     def h_copy(dz, d):
         return remote(hsend.at[d, dz], hall.at[d, dz], hs.at[d, dz], hr.at[d, dz], sp, lax.rem(me_x + d, 4))
@@ -336,21 +345,26 @@
             pltpu.make_async_copy(arrived, arrived, sr.at[dz]).wait()
             for way in range(2):
                 a_copy(dz, way).start()
-            after = GROUPS.index(dz) + LEAD
-            if after < 8:
-                dispatch(GROUPS[after])
+            if dz == GROUPS[-1]:
+                far_copy(dz).start()
+            for n in PACE[GROUPS.index(dz) + 1]:
+                dispatch(GROUPS[n])
 
     def stage_b(dz):
         with jax.named_scope(f"B{dz}"):
             for way in range(2):
                 a_copy(dz, way).wait()
-                b_copy(dz, way).start()
+                if dz != GROUPS[-1]:
+                    b_copy(dz, way).start()
 
     def stage_c(pair):
         with jax.named_scope(f"Cw{pair[0]}"):
             for dz in pair:
-                for way in range(2):
-                    b_copy(dz, way).wait()
+                if dz == GROUPS[-1]:
+                    far_copy(dz).wait()
+                else:
+                    for way in range(2):
+                        b_copy(dz, way).wait()
         with jax.named_scope(f"C{pair[0]}"):
             block = jnp.concatenate(
                 [recv[dz].reshape(24, 16, LANES) for dz in pair]
@@ -393,8 +407,6 @@
                     ret[0:3] = retsend[0, 0]
                 lax.fori_loop(1 if dz == 0 else 0, 8, give, 0)
 
-    pairs = [GROUPS[n:n + 2] for n in range(0, 8, 2)]
-
     def wait_down():
         with jax.named_scope("wait_down"):
             weights[3].wait()
@@ -404,34 +416,20 @@
 
     g = GROUPS
     stage_a(g[0])
-    stage_a(g[1])
-    stage_b(g[0])
-    stage_a(g[2])
-    stage_b(g[1])
-    stage_a(g[3])
-    stage_b(g[2])
-    weights[1].wait()
-    weights[2].wait()
-    stage_c(pairs[0])
-    stage_a(g[4])
-    stage_b(g[3])
-    stage_a(g[5])
-    stage_b(g[4])
-    wait_down()
-    stage_d(pairs[0])
-    stage_c(pairs[1])
-    stage_a(g[6])
-    stage_b(g[5])
-    stage_a(g[7])
-    stage_b(g[6])
-    stage_d(pairs[1])
-    stage_c(pairs[2])
-    stage_c(g[6:7])
-    stage_b(g[7])
-    stage_d(pairs[2])
-    stage_c(g[7:8])
-    stage_d(g[6:7])
-    stage_d(g[7:8])
+    for n in range(1, 11):
+        if n < 8:
+            stage_a(g[n])
+        if n == 2:
+            weights[1].wait()
+            weights[2].wait()
+        if n == 3:
+            wait_down()
+        if n <= 8:
+            stage_b(g[n - 1])
+        if 2 <= n <= 9:
+            stage_c(g[n - 2:n - 1])
+        if 3 <= n:
+            stage_d(g[n - 3:n - 2])
 
     with jax.named_scope("wait_ret"):
         pltpu.make_async_copy(ret.at[pl.ds(3, 189)], ret.at[pl.ds(3, 189)], tr).wait()

time: 99.1 us -> 98.3 us (level)
  no operation moved by 1% of the time
where the time goes in v5:
time: 98.3 us; the launch traced here: 98.2 us
  Pallas kernels  96.5 us (98%)
  local copies, waits for them, and re-layouts  1.67 us (2%)
    pallas_call x1, Pallas kernels, body(): pl.pallas_call(layer_kernel, out_shape=jax.ShapeDtypeStruct(resid_in.shap...  96.5 us

profile of v5, /device:TPU:1, one launch (start us, length us, event | category | flops | bytes accessed | tf_op | source)
XLA Modules:
  0.0 98.2 jit_solution(17624507564115731127)
XLA Ops:
  0.0 96.5 %shard_map.127 = bf16[64,2048]{1,0:T(8,128)(2,1)} custom-call(s32[2,256]{1,0:T(2,128)} %bitcast.14, f32[2,64]{1,0:T(2,128)} %bitcast.15, bf16[256,128]{1,0:T(8,128)(2,1)} %query_ref.1, bf16[64,256]{1,0:T(8,128)(2,1)} %bitcast.11, bf16[64,256]{1,0:T(8,128)(2,1)} %bitcast.12, f32[2,64]{1,0:T(2,128)} %qgain_ref.1, f32[1,64]{1,0:T(1,128)} %kgain_ref.1, ...), custom_call_target="tpu_custom_call" | custom-call | tf_op jit(solution)/shard_map/pallas_call | solution.py:468
  96.5 1.7 %copy.15 = bf16[64,2048]{1,0:T(8,128)(2,1)} copy(bf16[64,2048]{1,0:T(8,128)(2,1)} %shard_map.127) | data formatting | bytes 524288

commit v6 on v5

--- a/solution.py
+++ b/solution.py
@@ -20,7 +20,7 @@
 MESH = pl.DeviceIdType.MESH
 NEAR = (0, 1, 7, 2, 6, 3, 5, 4)
 PACE = ((0, 1, 2), (3,), (4,), (5,), (6,), (7,), (), (), ())
-GROUPS = (0, 1, 5, 3, 4, 6, 2, 7)
+GROUPS = (0, 1, 5, 4, 3, 6, 2, 7)
 PARTS = (((0, 512), (512, 256)), ((768, 512),), ((1280, 512), (1792, 256)))
 
 
@@ -61,9 +61,10 @@
 
 
 def layer_kernel(
-    ids_ref, route_ref, query_ref, key_ref, value_ref, qgain_ref, kgain_ref, resid_ref, gain_ref,
+    ids_in, route_in, query_in, key_in, value_in, qgain_in, kgain_in, resid_in, gain_in,
     outw_hbm, gate_hbm, up_hbm, down_hbm,
     out_ref,
+    ids_ref, route_ref, query_ref, key_ref, value_ref, qgain_ref, kgain_ref, resid_ref, gain_ref, isem,
     qall, kvall, kk, vt, best_s, acc_s, osend, mlsend, orecv, mlrecv, attv, att,
     outw, gatew, upw, dcat, pick, joiner, resid_s, sendbuf, recv, xall, hall, hsend, retsend, ret,
     wsem, qs, qr, ks, kr, ps, pr, ms, mr, xs, xr, ds, dr,
@@ -94,6 +95,14 @@
             for dz, dj in ((0, d), (d, 0)):
                 pl.semaphore_signal(barrier, inc=1, device_id=(at_offset(dz, dj), me_x), device_id_type=MESH)
 
+    small = [
+        pltpu.make_async_copy(a, b, isem.at[n])
+        for n, (a, b) in enumerate((
+            (query_in, query_ref), (key_in, key_ref), (value_in, value_ref), (qgain_in, qgain_ref),
+            (kgain_in, kgain_ref), (ids_in, ids_ref), (route_in, route_ref), (resid_in, resid_ref), (gain_in, gain_ref)))
+    ]
+    for copy in small:
+        copy.start()
     weights = [
         pltpu.make_async_copy(a, b, wsem.at[n])
         for n, (a, b) in enumerate(((outw_hbm, outw), (gate_hbm, gatew), (up_hbm, upw), (down_hbm, dcat.at[0])))
@@ -105,6 +114,8 @@
         lane = lax.broadcasted_iota(jnp.int32, (tok, LANES), 1)
         low = lane < HEAD_DIM
         cosine, sine_table = rotary_tables(sp)
+        for copy in small:
+            copy.wait()
         qgain = jnp.concatenate([qgain_ref[0:1, :], qgain_ref[1:2, :]], axis=1)
         qall[0] = prepare(query_ref[...].astype(f32), qgain, cosine, sine_table).astype(bf)
         key_value = jnp.concatenate([key_ref[...].astype(f32), value_ref[...].astype(f32)], axis=0).T
@@ -255,10 +266,6 @@
         return carry
 
     lax.fori_loop(0, 8, late, 0)
-    with jax.named_scope("down_turn"):
-        for way in range(2):
-            down_copy(way).wait()
-        pass_on(0)
 
     def finish(d, carry):
         ml_copy(d).wait()
@@ -290,7 +297,9 @@
     with jax.named_scope("x_exchange"):
         for d in (2, 1, 3):
             x_copy(d).start()
-        for n in range(1, 4):
+        for way in range(2):
+            down_copy(way).wait()
+        for n in range(4):
             pass_on(n)
         att[me_x] = attv[me_x]
         weights[0].wait()
@@ -332,10 +341,6 @@
             xall.at[2 * way, dz, part], xall.at[1, dz, part], bxs.at[way, dz], bxr.at[way, dz],
             sp, left if way == 0 else right)
 
-    def far_copy(dz):
-        return remote(
-            recv.at[dz], xall.at[1, dz], bxs.at[0, dz], bxr.at[0, dz], sp, lax.rem(me_x + 2, 4))
-
     def h_copy(dz, d):
         return remote(hsend.at[d, dz], hall.at[d, dz], hs.at[d, dz], hr.at[d, dz], sp, lax.rem(me_x + d, 4))
 
@@ -345,8 +350,6 @@
             pltpu.make_async_copy(arrived, arrived, sr.at[dz]).wait()
             for way in range(2):
                 a_copy(dz, way).start()
-            if dz == GROUPS[-1]:
-                far_copy(dz).start()
             for n in PACE[GROUPS.index(dz) + 1]:
                 dispatch(GROUPS[n])
 
@@ -354,17 +357,13 @@
         with jax.named_scope(f"B{dz}"):
             for way in range(2):
                 a_copy(dz, way).wait()
-                if dz != GROUPS[-1]:
-                    b_copy(dz, way).start()
+                b_copy(dz, way).start()
 
     def stage_c(pair):
         with jax.named_scope(f"Cw{pair[0]}"):
             for dz in pair:
-                if dz == GROUPS[-1]:
-                    far_copy(dz).wait()
-                else:
-                    for way in range(2):
-                        b_copy(dz, way).wait()
+                for way in range(2):
+                    b_copy(dz, way).wait()
         with jax.named_scope(f"C{pair[0]}"):
             block = jnp.concatenate(
                 [recv[dz].reshape(24, 16, LANES) for dz in pair]
@@ -468,9 +467,19 @@
     return pl.pallas_call(
         layer_kernel,
         out_shape=jax.ShapeDtypeStruct(resid_in.shape, bf),
-        in_specs=[vmem] * 9 + [hbm] * 4,
+        in_specs=[hbm] * 13,
         out_specs=vmem,
         scratch_shapes=[
+            pltpu.VMEM((TOPK, tok), jnp.int32),
+            pltpu.VMEM((TOPK, rows), f32),
+            pltpu.VMEM(query_proj.shape, bf),
+            pltpu.VMEM(key_proj.shape[::-1], bf),
+            pltpu.VMEM(value_proj.shape[::-1], bf),
+            pltpu.VMEM(query_gain.shape, f32),
+            pltpu.VMEM(key_gain.shape, f32),
+            pltpu.VMEM(resid_in.shape, bf),
+            pltpu.VMEM((1,) + norm_gain.shape, f32),
+            dma((9,)),
             pltpu.VMEM((8, tok, LANES), bf),
             pltpu.VMEM((8, tok, LANES), bf),
             pltpu.VMEM((8 * tok, LANES), bf),
@@ -500,7 +509,7 @@
         ] + [dma((4,))] + [dma((8,))] * 8 + [dma((4,))] * 2 + [dma((10,))] * 2
         + [dma(()), dma((8,))] + [dma((2, 8))] * 4 + [dma((4, 8))] * 2 + [dma(())] * 2,
         compiler_params=pltpu.CompilerParams(
-            collective_id=0, has_side_effects=True, vmem_limit_bytes=60 << 20),
+            collective_id=0, has_side_effects=True, vmem_limit_bytes=67_000_000),
     )(
         expert_ids.T, route_weight.T, query_proj, key_proj.T, value_proj.T, query_gain, key_gain, resid_in,
         norm_gain[None], out_weight, gate_weight[0], up_weight[0], down_weight[0],

time: 98.3 us -> 96.3 us (0.980)
  Pallas kernels: 96.5 us -> 94.5 us
    pallas_call x1, Pallas kernels: 96.5 us -> 94.5 us  [body(): pl.pallas_call(layer_kernel, out_shape=jax.ShapeDtypeStruct(resid_in.shap...]
where the time goes in v6:
time: 96.3 us; the launch traced here: 96.2 us
  Pallas kernels  94.5 us (98%)
  local copies, waits for them, and re-layouts  1.67 us (2%)
    pallas_call x1, Pallas kernels, body(): pl.pallas_call(layer_kernel, out_shape=jax.ShapeDtypeStruct(resid_in.shap...  94.5 us

profile of v6, /device:TPU:1, one launch (start us, length us, event | category | flops | bytes accessed | tf_op | source)
XLA Modules:
  0.0 96.2 jit_solution(16572332668293488772)
XLA Ops:
  0.0 94.5 %shard_map.127 = bf16[64,2048]{1,0:T(8,128)(2,1)} custom-call(s32[2,256]{1,0:T(2,128)} %bitcast.14, f32[2,64]{1,0:T(2,128)} %bitcast.15, bf16[256,128]{1,0:T(8,128)(2,1)} %query_in.1, bf16[64,256]{1,0:T(8,128)(2,1)} %bitcast.11, bf16[64,256]{1,0:T(8,128)(2,1)} %bitcast.12, f32[2,64]{1,0:T(2,128)} %qgain_in.1, f32[1,64]{1,0:T(1,128)} %kgain_in.1, ...), custom_call_target="tpu_custom_call" | custom-call | tf_op jit(solution)/shard_map/pallas_call | solution.py:467
  94.5 1.7 %copy.15 = bf16[64,2048]{1,0:T(8,128)(2,1)} copy(bf16[64,2048]{1,0:T(8,128)(2,1)} %shard_map.127) | data formatting | bytes 524288

commit v7 on v6

--- a/solution.py
+++ b/solution.py
@@ -19,7 +19,7 @@
 LANES = 128
 MESH = pl.DeviceIdType.MESH
 NEAR = (0, 1, 7, 2, 6, 3, 5, 4)
-PACE = ((0, 1, 2), (3,), (4,), (5,), (6,), (7,), (), (), ())
+PACE = ((0, 1, 2), (3, 4), (5,), (6,), (7,), (), (), (), ())
 GROUPS = (0, 1, 5, 4, 3, 6, 2, 7)
 PARTS = (((0, 512), (512, 256)), ((768, 512),), ((1280, 512), (1792, 256)))
 

time: 96.3 us -> 96.3 us (level)
  no operation moved by 1% of the time
where the time goes in v7:
time: 96.3 us; the launch traced here: 96.2 us
  Pallas kernels  94.5 us (98%)
  local copies, waits for them, and re-layouts  1.67 us (2%)
    pallas_call x1, Pallas kernels, body(): pl.pallas_call(layer_kernel, out_shape=jax.ShapeDtypeStruct(resid_in.shap...  94.5 us

profile of v7, /device:TPU:1, one launch (start us, length us, event | category | flops | bytes accessed | tf_op | source)
XLA Modules:
  0.0 96.2 jit_solution(6944314784016077123)
XLA Ops:
  0.0 94.5 %shard_map.127 = bf16[64,2048]{1,0:T(8,128)(2,1)} custom-call(s32[2,256]{1,0:T(2,128)} %bitcast.14, f32[2,64]{1,0:T(2,128)} %bitcast.15, bf16[256,128]{1,0:T(8,128)(2,1)} %query_in.1, bf16[64,256]{1,0:T(8,128)(2,1)} %bitcast.11, bf16[64,256]{1,0:T(8,128)(2,1)} %bitcast.12, f32[2,64]{1,0:T(2,128)} %qgain_in.1, f32[1,64]{1,0:T(1,128)} %kgain_in.1, ...), custom_call_target="tpu_custom_call" | custom-call | tf_op jit(solution)/shard_map/pallas_call | solution.py:467
  94.5 1.7 %copy.15 = bf16[64,2048]{1,0:T(8,128)(2,1)} copy(bf16[64,2048]{1,0:T(8,128)(2,1)} %shard_map.127) | data formatting | bytes 524288
